TPU v7x, 256 devices: a 4x2x16 block of a 4x16x16 slice. The times are simulated.
256 devices in a mesh: grp: 2 (over y), kv: 32 (over z, core), tp: 4 (over x).
Axes of the slice: x: 4, y: 2, z: 16, core: 2. Of those that a mesh axis runs over, the one named last changes fastest.
The devices are a block of a 4x16x16 slice.
Arguments:
- tokens: bfloat16 [16, 4096], P('grp', ('kv', 'tp')), parts along dimension 0, may hold values from -6 to 6
- input_gain: float32 [4096], P(('kv', 'tp')), may hold values from 0.1 to 1.9
- query_down: bfloat16 [4096, 1536], P(('kv', 'tp')), may hold values from -0.09375 to 0.09375
- latent_down: bfloat16 [4096, 1056], P(('kv', 'tp')), may hold values from -0.09375 to 0.09375
- query_gain: float32 [1536], replicated, may hold values from 0.1 to 1.9
- query_up: bfloat16 [1536, 3072], P('kv', 'tp'), may hold values from -0.15625 to 0.15625
- nope_gain: float32 [64], replicated, may hold values from 0.1 to 1.9
- query_rope_gain: float32 [32], replicated, may hold values from 0.1 to 1.9
- key_up: bfloat16 [1024, 2048], P('kv', 'tp'), may hold values from -0.1875 to 0.1875
- latent_gain: float32 [1024], replicated, may hold values from 0.1 to 1.9
- key_rope_gain: float32 [32], replicated, may hold values from 0.1 to 1.9
- latent_cache: bfloat16 [16, 12288, 1024], P('grp', 'kv'), parts along dimension 0, may hold values from -270 to 270
- rope_cache: bfloat16 [16, 32, 12288], P('grp', None, 'kv'), parts along dimension 0, may hold values from -4 to 4
- lengths: int32 [16], P('grp'), parts along dimension 0, may hold values from 3072 to 12288, as said below
- value_up: bfloat16 [1024, 2048], P('kv', 'tp'), may hold values from -6 to 6
- output_proj: bfloat16 [2048, 4096], P('tp', 'kv'), may hold values from -0.125 to 0.125
Outputs:
- attended: bfloat16 [16, 4096], P('grp', ('kv', 'tp')), parts along dimension 0
- new_latent: bfloat16 [16, 1024], P('grp'), parts along dimension 0
- new_rope_key: bfloat16 [16, 32], P('grp'), parts along dimension 0
There are 2 independent parts, one for each index of `grp`. A program takes and returns all parts, laid end to end along the dimension named above; an argument that names none is the same for every part. Nothing has to cross between parts.
Inputs may be any that keep to these rules, and one draw needn't show every extreme that they name: Positions below a sequence's length hold its cache; the new token stands at position lengths; one sequence has length 12288 and one a quarter of 12288.
All inputs are finite; a program needn't handle non-finite values.
Results may differ from a plain program's by a relative error of at most 0.03.
Values may be sent and summed in bfloat16 or wider, within the bound.
No kernel may reach another device: no remote copies, remote signals or barrier semaphores. Data moves between devices by JAX's collectives and lax.ppermute only.
A program may use at most 64 MiB of HBM per device.

v0:
```python
import functools

import jax
import jax.numpy as jnp
from jax import lax
from jax.sharding import Mesh
from jax.sharding import PartitionSpec as P

D = 4096
KV_RANK = 1024
NOPE = 64
ROPE = 32
VDIM = 64
KV_TP = ("kv_0", "kv_1", "tp")
KV = ("kv_0", "kv_1")


epsilon = 1e-06
theta = 10000.0
lowest = -1e30


def one_axis_at_a_time(x, axes):
    return functools.reduce(lax.psum, axes, x)


def joined_along(tiles, dim):
    tiles = jnp.moveaxis(tiles, 0, dim)
    dims = tiles.shape
    return tiles.reshape(*dims[:dim], dims[dim] * dims[dim + 1], *dims[dim + 2 :])


def sent_to_all(x, axis):
    devices = lax.axis_size(axis)
    return lax.all_to_all(jnp.broadcast_to(x[None], (devices, *x.shape)), axis, 0, 0, tiled=True)


def gather_directly(x, axis, dim):
    return joined_along(sent_to_all(x, axis), dim)


def of_everyone(x, axis):
    return sent_to_all(x, axis).max(axis=0)


def cut_along(x, dim, devices):
    dims = x.shape
    tiles = x.reshape(*dims[:dim], devices, dims[dim] // devices, *dims[dim + 1 :])
    return jnp.moveaxis(tiles, dim, 0)


def summed_on_arrival(x, axis, dim):
    tiles = cut_along(x, dim, lax.axis_size(axis))
    arrived = lax.all_to_all(tiles, axis, split_axis=0, concat_axis=0, tiled=True)
    return arrived.astype(jnp.float32).sum(axis=0)


def over_copies(x, axis):
    everything = sent_to_all(x, axis)
    return jnp.sum(everything, axis=0)


def normalize(values, gain):
    return values * lax.rsqrt(jnp.mean(values * values, axis=-1, keepdims=True) + epsilon) * gain


def rotate(values, positions):
    half_width = values.shape[-1] // 2
    frequency = theta ** (-jnp.arange(half_width, dtype=jnp.float32) / half_width)
    angles = (
        positions.astype(jnp.float32).reshape(positions.shape + (1,) * (values.ndim - 1))
        * frequency
    )
    cosines = jnp.cos(angles)
    sines = jnp.sin(angles)
    upper = values[..., :half_width]
    lower = values[..., half_width:]
    return jnp.concatenate(
        [upper * cosines - lower * sines, upper * sines + lower * cosines], axis=-1
    )


def body(
    tokens,
    input_gain,
    query_down,
    latent_down,
    query_gain,
    query_up,
    nope_gain,
    query_rope_gain,
    key_up,
    latent_gain,
    key_rope_gain,
    latent_cache,
    rope_cache,
    lengths,
    value_up,
    output_proj,
):
    batch_size = tokens.shape[0]
    floats = tokens.astype(jnp.float32)
    scaled = (floats * input_gain).astype(jnp.bfloat16)
    squares, query_low, latent_low = (
        one_axis_at_a_time(jnp.sum(floats * floats, axis=1), KV_TP),
        one_axis_at_a_time(jnp.dot(scaled, query_down, preferred_element_type=jnp.float32), KV_TP),
        one_axis_at_a_time(jnp.dot(scaled, latent_down, preferred_element_type=jnp.float32), KV_TP),
    )
    inverse = lax.rsqrt(squares / D + epsilon)[:, None]
    query_lat = normalize(query_low * inverse, query_gain).astype(jnp.bfloat16)
    latent_low = latent_low * inverse
    new_latent = normalize(latent_low[:, :KV_RANK], latent_gain).astype(jnp.bfloat16)
    new_rope_key = rotate(normalize(latent_low[:, KV_RANK:], key_rope_gain), lengths).astype(
        jnp.bfloat16
    )
    kv_index = lax.axis_index(KV)
    row_count = query_up.shape[0]
    own_rows = lax.dynamic_slice_in_dim(query_lat, kv_index * row_count, row_count, 1)
    head_count = query_up.shape[1] // (NOPE + ROPE)
    queries = one_axis_at_a_time(
        jnp.dot(own_rows, query_up, preferred_element_type=jnp.float32), KV
    ).reshape(batch_size, head_count, NOPE + ROPE)
    query_nope = normalize(queries[..., :NOPE], nope_gain).astype(jnp.bfloat16)
    query_rope = rotate(normalize(queries[..., NOPE:], query_rope_gain), lengths).astype(
        jnp.bfloat16
    )
    key_rows = key_up.shape[0]
    latent_part = jnp.einsum(
        "bhd,rhd->bhr",
        query_nope,
        key_up.reshape(key_rows, head_count, NOPE),
        preferred_element_type=jnp.float32,
    ).astype(jnp.bfloat16)
    query_latent = gather_directly(latent_part, KV, 2)
    score_scale = (NOPE + ROPE) ** (-0.5)
    context_rows = latent_cache.shape[1]
    positions = kv_index * context_rows + jnp.arange(context_rows, dtype=jnp.int32)
    usable = (positions[None, :] < lengths[:, None])[:, None, :]
    scores = (
        jnp.einsum("bhr,bpr->bhp", query_latent, latent_cache, preferred_element_type=jnp.float32)
        + jnp.einsum("bhd,bdp->bhp", query_rope, rope_cache, preferred_element_type=jnp.float32)
    ) * score_scale
    fresh = (
        jnp.einsum("bhr,br->bh", query_latent, new_latent, preferred_element_type=jnp.float32)
        + jnp.einsum("bhd,bd->bh", query_rope, new_rope_key, preferred_element_type=jnp.float32)
    ) * score_scale
    leader = kv_index == 0
    masked = jnp.where(usable, scores, lowest)
    local_top = jnp.maximum(jnp.max(masked, axis=2), jnp.where(leader, fresh, lowest))
    weights = jnp.where(usable, jnp.exp(masked - local_top[..., None]), 0.0)
    fresh_weight = jnp.where(leader, jnp.exp(fresh - local_top), 0.0)
    totals = jnp.sum(weights, axis=2) + fresh_weight
    rounded_fresh = lax.optimization_barrier(fresh_weight.astype(jnp.bfloat16)).astype(jnp.float32)
    summed = (
        jnp.einsum(
            "bhp,bpr->bhr",
            weights.astype(jnp.bfloat16),
            latent_cache,
            preferred_element_type=jnp.float32,
        )
        + rounded_fresh[..., None] * new_latent.astype(jnp.float32)[:, None, :]
    )
    value_rows = value_up.shape[0]
    top = of_everyone(local_top, KV)
    factor = jnp.exp(local_top - top)
    copies = jnp.broadcast_to((totals * factor)[..., None], totals.shape + (lax.axis_size(KV),))
    shares, share_totals = (
        summed_on_arrival((summed * factor[..., None]).astype(jnp.bfloat16), KV, 2),
        summed_on_arrival(copies.astype(jnp.bfloat16), KV, 2),
    )
    latent_out = (shares / share_totals).astype(jnp.bfloat16)
    head_part = jnp.einsum(
        "bhr,rhe->bhe",
        latent_out,
        value_up.reshape(value_rows, head_count, VDIM),
        preferred_element_type=jnp.float32,
    ).reshape(batch_size, head_count * VDIM)
    head_out = over_copies(head_part, KV).astype(jnp.bfloat16)
    partial_value = jnp.dot(head_out, output_proj, preferred_element_type=jnp.float32)
    attended = summed_on_arrival(partial_value.astype(jnp.bfloat16), "tp", 1).astype(jnp.bfloat16)
    return (attended, new_latent, new_rope_key)


def solution(mesh):
    split = Mesh(
        mesh.devices.reshape(mesh.shape["grp"], 16, 2, mesh.shape["tp"]),
        ("grp", "kv_0", "kv_1", "tp"),
    )
    placed = (
        P("grp", KV_TP),
        P(KV_TP),
        P(KV_TP, None),
        P(KV_TP, None),
        P(),
        P(KV, "tp"),
        P(),
        P(),
        P(KV, "tp"),
        P(),
        P(),
        P("grp", KV, None),
        P("grp", None, KV),
        P("grp"),
        P(KV, "tp"),
        P("tp", KV),
    )
    return jax.shard_map(
        body,
        mesh=split,
        in_specs=placed,
        out_specs=(P("grp", KV_TP), P("grp", None), P("grp", None)),
        check_vma=False,
    )
```

profile of v0, /device:TPU:40, one launch (start us, length us, event | category | flops | bytes accessed | tf_op | source)
XLA Modules:
  0.0 310.0 jit_solution(700729327897130116)
XLA Ops:
  0.7 0.8 fusion.19
  1.5 1.1 fusion.30
  2.5 75.0 %all-reduce.1 = (f32[8,1536]{1,0:T(8,128)S(1)}, f32[8]{0:T(128)S(1)}) all-reduce(f32[8,1536]{1,0:T(8,128)S(1)} %fusion.30, f32[8]{0:T(128)S(1)} %fusion.19), channel_id=1, replica_groups=mesh['grp'=2,'kv_0'=16,'kv_1'=2,'tp'=4] {'kv_0'}, use_global_device_ids=true, to_apply=%region_0.0 | all-reduce | flops 12296 | bytes 98368 | tf_op jit(solution)/shard_map/psum | solution.py:24
  77.6 3.6 %all-reduce.4 = (f32[8,1536]{1,0:T(8,128)S(1)}, f32[8]{0:T(128)S(1)}) all-reduce(f32[8,1536]{1,0:T(8,128)S(1)} %get-tuple-element.5, f32[8]{0:T(128)S(1)} %get-tuple-element.6), channel_id=1, replica_groups=mesh['grp'=2,'kv_0'=16,'kv_1'=2,'tp'=4] {'kv_1'}, use_global_device_ids=true, to_apply=%region_1.0 | all-reduce | flops 12296 | bytes 98368 | tf_op jit(solution)/shard_map/psum | solution.py:24
  81.2 18.0 %all-reduce.2 = (f32[8,1536]{1,0:T(8,128)S(1)}, f32[8]{0:T(128)S(1)}) all-reduce(f32[8,1536]{1,0:T(8,128)S(1)} %get-tuple-element.11, f32[8]{0:T(128)S(1)} %get-tuple-element.12), channel_id=1, replica_groups=mesh['grp'=2,'kv_0'=16,'kv_1'=2,'tp'=4] {'tp'}, use_global_device_ids=true, to_apply=%region_2.0 | all-reduce | flops 12296 | bytes 98368 | tf_op jit(solution)/shard_map/psum | solution.py:24
  99.4 1.0 fusion.28
  100.4 0.8 dynamic-slice
  101.2 1.1 fusion.24
  102.3 52.9 %all-reduce = (f32[8,768]{1,0:T(8,128)S(1)}, f32[8,1056]{1,0:T(8,128)S(1)}) all-reduce(f32[8,768]{1,0:T(8,128)S(1)} %fusion.24, f32[8,1056]{1,0:T(8,128)S(1)} %fusion.28), channel_id=1, replica_groups=mesh['grp'=2,'kv_0'=16,'kv_1'=2,'tp'=4] {'kv_0'}, use_global_device_ids=true, to_apply=%region_8.0 | all-reduce | flops 14592 | bytes 116736 | tf_op jit(solution)/shard_map/psum | solution.py:24
  155.3 3.6 %all-reduce.3 = (f32[8,8,96]{2,1,0:T(8,128)S(1)}, f32[8,1056]{1,0:T(8,128)S(1)}) all-reduce(f32[8,8,96]{2,1,0:T(8,128)S(1)} %reshape.178, f32[8,1056]{1,0:T(8,128)S(1)} %get-tuple-element.4), channel_id=1, replica_groups=mesh['grp'=2,'kv_0'=16,'kv_1'=2,'tp'=4] {'kv_1'}, use_global_device_ids=true, to_apply=%region_9.0 | all-reduce | flops 14592 | bytes 116736 | tf_op jit(solution)/shard_map/psum | solution.py:24
  158.9 0.9 reshape.179
  159.8 0.7 multiply_convert_fusion.1
  160.8 1.2 reshape.188
  162.0 4.8 %all-to-all-start = ((bf16[32,2,1024]{2,1,0:T(2,128)(2,1)}), bf16[32,2,1024]{2,1,0:T(2,128)(2,1)S(1)}, u32[]{:S(2)}, u32[]{:S(2)}) async-start(bf16[32,2,1024]{2,1,0:T(2,128)(2,1)} %reshape.188), calls=%async_computation | async-start | bytes 262144 | tf_op jit(solution)/shard_map/all_to_all | solution.py:35
  167.0 14.7 %psum.87 = f32[8,1056]{1,0:T(8,128)S(1)} all-reduce(f32[8,1056]{1,0:T(8,128)S(1)} %get-tuple-element.10), channel_id=1, replica_groups=mesh['grp'=2,'kv_0'=16,'kv_1'=2,'tp'=4] {'tp'}, use_global_device_ids=true, to_apply=%region_15.0 | all-reduce | flops 8448 | bytes 67584 | tf_op jit(solution)/shard_map/psum | solution.py:24
  182.7 0.7 broadcast_compare_fusion
  183.4 0.7 multiply_multiply_fusion.1
  184.1 0.7 multiply_multiply_fusion
  185.4 0.8 fusion.36
  187.5 4.5 %fusion.38 = f32[8,8,384]{2,1,0:T(8,128)S(1)} fusion(bf16[8,8,1024]{2,1,0:T(8,128)(2,1)S(1)} %reshape.180, bf16[8,384,1024]{2,1,0:T(8,128)(2,1)} %param.27), kind=kOutput, calls=%fused_computation.81 | convolution fusion | flops 50331648 | bytes 6520832 | tf_op jit(solution)/shard_map/bhr,bpr->bhp/dot_general | solution.py:140
  193.0 12.4 %all-to-all-start.1 = ((f32[32,8,8]{2,1,0:T(8,128)}), f32[32,8,8]{2,1,0:T(8,128)S(1)}, u32[]{:S(2)}, u32[]{:S(2)}) async-start(f32[32,8,8]{2,1,0:T(8,128)} %broadcast_in_dim.39), calls=%async_computation.1 | async-start | bytes 262144 | tf_op jit(solution)/shard_map/all_to_all | solution.py:35
  205.5 16.3 %all-to-all-done.1 = f32[32,8,8]{2,1,0:T(8,128)S(1)} async-done(((f32[32,8,8]{2,1,0:T(8,128)}), f32[32,8,8]{2,1,0:T(8,128)S(1)}, u32[]{:S(2)}, u32[]{:S(2)}) %all-to-all-start.1) | async-done | bytes 8224 | tf_op jit(solution)/shard_map/all_to_all | solution.py:35
  222.6 4.8 %all-to-all-start.3 = ((bf16[32,8,8,1]{2,1,3,0:T(8,128)(2,1)}), bf16[32,8,8,1]{2,1,3,0:T(8,128)(2,1)S(1)}, u32[]{:S(2)}, u32[]{:S(2)}) async-start(bf16[32,8,8,1]{2,1,3,0:T(8,128)(2,1)} %transpose.55), calls=%async_computation.3 | async-start | bytes 131072 | tf_op jit(solution)/shard_map/all_to_all | solution.py:54
  227.4 3.8 %fusion.1 = bf16[8,8,1024]{2,1,0:T(8,128)(2,1)S(1)} fusion(bf16[8,384,1024]{2,1,0:T(8,128)(2,1)} %param.27, f32[8,8]{1,0:T(8,128)S(1)} %get-tuple-element.15, f32[8,1024]{1,0:T(8,128)S(1)} %get-tuple-element.16, f32[8,8]{1,0:T(8,128)S(1)} %convert_element_type.73, f32[8,8,384]{2,1,0:T(8,128)S(1)} %get-tuple-element.27, f32[8,8]{1,0:T(8,128)S(1)} %select_maximum_fusion, ...), kind=kOutput, calls=%fused_computation.2 | convolution fusion | flops 50667520 | bytes 6557440 | tf_op jit(solution)/shard_map/bhp,bpr->bhr/dot_general | solution.py:155
  231.7 1.2 reshape.190
  232.9 8.0 %all-to-all-done.3 = bf16[32,8,8,1]{2,1,3,0:T(8,128)(2,1)S(1)} async-done(((bf16[32,8,8,1]{2,1,3,0:T(8,128)(2,1)}), bf16[32,8,8,1]{2,1,3,0:T(8,128)(2,1)S(1)}, u32[]{:S(2)}, u32[]{:S(2)}) %all-to-all-start.3) | async-done | bytes 4128 | tf_op jit(solution)/shard_map/all_to_all | solution.py:54
  240.9 4.8 %all-to-all-start.2 = ((bf16[32,2,1024]{2,1,0:T(2,128)(2,1)}), bf16[32,2,1024]{2,1,0:T(2,128)(2,1)S(1)}, u32[]{:S(2)}, u32[]{:S(2)}) async-start(bf16[32,2,1024]{2,1,0:T(2,128)(2,1)} %reshape.190), calls=%async_computation.2 | async-start | bytes 262144 | tf_op jit(solution)/shard_map/all_to_all | solution.py:54
  245.8 16.2 %all-to-all-done.2 = bf16[32,2,1024]{2,1,0:T(2,128)(2,1)S(1)} async-done(((bf16[32,2,1024]{2,1,0:T(2,128)(2,1)}), bf16[32,2,1024]{2,1,0:T(2,128)(2,1)S(1)}, u32[]{:S(2)}, u32[]{:S(2)}) %all-to-all-start.2) | async-done | bytes 131104 | tf_op jit(solution)/shard_map/all_to_all | solution.py:54
  262.8 37.1 %all_to_all.30 = f32[32,8,512]{2,1,0:T(8,128)S(1)} all-to-all(f32[32,8,512]{2,1,0:T(8,128)S(1)} %broadcast_in_dim.41), channel_id=1, replica_groups=mesh['grp'=2,'kv_0'=16,'kv_1'=2,'tp'=4] {'kv_0','kv_1'}, dimensions={0} | all-to-all | bytes 1048576 | tf_op jit(solution)/shard_map/all_to_all | solution.py:35
  300.2 0.7 reshape.192
  300.8 3.3 %all-to-all-start.5 = ((bf16[4,2,128]{2,1,0:T(2,128)(2,1)}), bf16[4,2,128]{2,1,0:T(2,128)(2,1)S(1)}, u32[]{:S(2)}, u32[]{:S(2)}) async-start(bf16[4,2,128]{2,1,0:T(2,128)(2,1)} %reshape.192), calls=%async_computation.5 | async-start | bytes 4096 | tf_op jit(solution)/shard_map/all_to_all | solution.py:54
  304.8 4.5 %all-to-all-done.5 = bf16[4,2,128]{2,1,0:T(2,128)(2,1)S(1)} async-done(((bf16[4,2,128]{2,1,0:T(2,128)(2,1)}), bf16[4,2,128]{2,1,0:T(2,128)(2,1)S(1)}, u32[]{:S(2)}, u32[]{:S(2)}) %all-to-all-start.5) | async-done | bytes 2080 | tf_op jit(solution)/shard_map/all_to_all | solution.py:54
  (62 shorter events, 8.5 us)
Async XLA Ops:
  0.6 191.4 %copy-start = (bf16[8,32,384]{2,1,0:T(8,128)(2,1)S(1)}, bf16[8,32,384]{2,1,0:T(8,128)(2,1)}, u32[]{:S(2)}) copy-start(bf16[8,32,384]{2,1,0:T(8,128)(2,1)} %param.28) | copy-start | bytes 589828
  162.0 24.1 %all-to-all-start = ((bf16[32,2,1024]{2,1,0:T(2,128)(2,1)}), bf16[32,2,1024]{2,1,0:T(2,128)(2,1)S(1)}, u32[]{:S(2)}, u32[]{:S(2)}) async-start(bf16[32,2,1024]{2,1,0:T(2,128)(2,1)} %reshape.188), calls=%async_computation | async-start | bytes 262144 | tf_op jit(solution)/shard_map/all_to_all | solution.py:35
  186.1 45.0 %copy-start.3 = (bf16[8,1024]{1,0:T(8,128)(2,1)}, bf16[8,1024]{1,0:T(8,128)(2,1)S(1)}, u32[]{:S(2)}) copy-start(bf16[8,1024]{1,0:T(8,128)(2,1)S(1)} %get-tuple-element.17) | copy-start | bytes 49156
  193.0 28.9 %all-to-all-start.1 = ((f32[32,8,8]{2,1,0:T(8,128)}), f32[32,8,8]{2,1,0:T(8,128)S(1)}, u32[]{:S(2)}, u32[]{:S(2)}) async-start(f32[32,8,8]{2,1,0:T(8,128)} %broadcast_in_dim.39), calls=%async_computation.1 | async-start | bytes 262144 | tf_op jit(solution)/shard_map/all_to_all | solution.py:35
  222.6 18.4 %all-to-all-start.3 = ((bf16[32,8,8,1]{2,1,3,0:T(8,128)(2,1)}), bf16[32,8,8,1]{2,1,3,0:T(8,128)(2,1)S(1)}, u32[]{:S(2)}, u32[]{:S(2)}) async-start(bf16[32,8,8,1]{2,1,3,0:T(8,128)(2,1)} %transpose.55), calls=%async_computation.3 | async-start | bytes 131072 | tf_op jit(solution)/shard_map/all_to_all | solution.py:54
  227.3 18.4 %copy-start.2 = (bf16[32,512]{1,0:T(8,128)(2,1)S(1)}, bf16[32,512]{1,0:T(8,128)(2,1)}, u32[]{:S(2)}) copy-start(bf16[32,512]{1,0:T(8,128)(2,1)} %param.30) | copy-start | bytes 98308
  227.3 72.6 %copy-start.1 = (bf16[512,128]{1,0:T(8,128)(2,1)S(1)}, bf16[512,128]{1,0:T(8,128)(2,1)}, u32[]{:S(2)}) copy-start(bf16[512,128]{1,0:T(8,128)(2,1)} %param.31) | copy-start | bytes 393220
  240.9 21.1 %all-to-all-start.2 = ((bf16[32,2,1024]{2,1,0:T(2,128)(2,1)}), bf16[32,2,1024]{2,1,0:T(2,128)(2,1)S(1)}, u32[]{:S(2)}, u32[]{:S(2)}) async-start(bf16[32,2,1024]{2,1,0:T(2,128)(2,1)} %reshape.190), calls=%async_computation.2 | async-start | bytes 262144 | tf_op jit(solution)/shard_map/all_to_all | solution.py:54
  300.8 8.5 %all-to-all-start.5 = ((bf16[4,2,128]{2,1,0:T(2,128)(2,1)}), bf16[4,2,128]{2,1,0:T(2,128)(2,1)S(1)}, u32[]{:S(2)}, u32[]{:S(2)}) async-start(bf16[4,2,128]{2,1,0:T(2,128)(2,1)} %reshape.192), calls=%async_computation.5 | async-start | bytes 4096 | tf_op jit(solution)/shard_map/all_to_all | solution.py:54
where the time goes:
time: 311 us; the launch traced here: 310 us
  blocking collectives  205 us (66%)
  waiting for transfers between devices  45.1 us (15%)
  starting transfers between devices  30 us (10%)
  matrix products  12.6 us (4%)
  local copies, waits for them, and re-layouts  8.54 us (3%)
  other arithmetic  8 us (3%)
    psum x6, blocking collectives, one_axis_at_a_time(): return functools.reduce(lax.psum, axes, x)  168 us
    all_to_all x1, blocking collectives, sent_to_all(): lax.all_to_all(jnp.broadcast_to(x[None], (devices, *x.shape)), axis, 0, 0...  37.1 us
    all_to_all x3, waiting for transfers between devices, summed_on_arrival(): lax.all_to_all(tiles, axis, split_axis=0, concat_axis=0, tiled=True)  28.8 us
    all_to_all x2, starting transfers between devices, sent_to_all(): lax.all_to_all(jnp.broadcast_to(x[None], (devices, *x.shape)), axis, 0, 0...  17.2 us
    all_to_all x2, waiting for transfers between devices, sent_to_all(): lax.all_to_all(jnp.broadcast_to(x[None], (devices, *x.shape)), axis, 0, 0...  16.3 us
    all_to_all x3, starting transfers between devices, summed_on_arrival(): lax.all_to_all(tiles, axis, split_axis=0, concat_axis=0, tiled=True)  12.8 us
  transfers between devices with their start and end apart: 5, of which 4 were waited for; matrix products, arithmetic and copies ran while one was open for 4% of the time, Pallas kernels for 0%

commit v1 on v0

v1 whole, which is shorter than its diff:
```python
import jax
import jax.numpy as jnp
from jax import lax
from jax.experimental import pallas as pl
from jax.experimental.pallas import tpu as pltpu
from jax.sharding import Mesh
from jax.sharding import PartitionSpec as P

NOPE = 64
ROPE = 32
VDIM = 64
LANES = 128
KV = ("hi", "lo")
KV_TP = ("hi", "lo", "tp")

epsilon = 1e-06
theta = 10000.0
lowest = -1e30

f32 = jnp.float32
bf16 = jnp.bfloat16

IN_VMEM = pl.BlockSpec(memory_space=pltpu.VMEM)
IN_SMEM = pl.BlockSpec(memory_space=pltpu.SMEM)


def run(kernel, outs, *args, scratch=(), smem=()):
    return pl.pallas_call(
        kernel,
        out_shape=outs,
        in_specs=[IN_SMEM if i in smem else IN_VMEM for i in range(len(args))],
        out_specs=jax.tree.map(lambda _: IN_VMEM, outs),
        scratch_shapes=scratch,
    )(*args)


def exchange(x, axes):
    return lax.all_to_all(x, axes, 0, 0, tiled=True)


def from_others(x, axis):
    n = lax.axis_size(axis)
    return [lax.ppermute(x, axis, [(i, (i + s) % n) for i in range(n)]) for s in range(1, n)]


def lane_of(rows):
    return lax.broadcasted_iota(jnp.int32, (rows, LANES), 1)


def shifted(x, amount):
    return pltpu.roll(x, amount % LANES, 1) if amount % LANES else x


def window(x, start, length):
    tile, off = divmod(start, LANES)
    first = shifted(x[:, tile * LANES : (tile + 1) * LANES], -off)
    if off + length <= LANES:
        return first
    second = shifted(x[:, (tile + 1) * LANES : (tile + 2) * LANES], -off)
    return jnp.where(lane_of(x.shape[0]) < LANES - off, first, second)


def swapped_halves(x):
    half = ROPE // 2
    return jnp.where(lane_of(x.shape[0]) % ROPE < half, shifted(x, -half), shifted(x, half))


def split_two(x):
    top = x.astype(bf16).astype(f32)
    return top, (x - top).astype(bf16).astype(f32)


def dot(a, b):
    return jnp.dot(a, b, preferred_element_type=f32)


def compress(tokens, gain, query_down, latent_down, key_up, value_up, out, by_batch):
    kv, batch = out.shape[0], tokens.shape[0]
    heads = by_batch.shape[0]
    own = query_down.shape[1] // kv
    half = key_up.shape[0] // 2
    values = tokens[...].astype(f32)
    scaled = (values * gain[...]).astype(bf16)
    squares = jnp.sum(values * values, axis=1, keepdims=True)
    part_q = dot(scaled, query_down[...])
    part_l = dot(scaled, latent_down[...])
    lane = lane_of(batch)
    rest = jnp.concatenate([part_l[:, 8 * LANES :], jnp.zeros((batch, LANES - ROPE), f32)], axis=1)
    fixed = jnp.where(lane < 2 * ROPE, squares, shifted(rest, 2 * ROPE))
    for k in range(kv):
        out[k, 0:8, :] = jnp.where(lane < own, window(part_q, own * k, own), fixed).astype(bf16)
    for j in range(8):
        by_batch[:, j, :] = part_l[:, j * LANES : (j + 1) * LANES]
    for n in range(heads):
        tile = by_batch[n].astype(bf16)
        for k in range(n, kv, heads):
            out[k, 8:16, :] = tile
    low_lane = lane_of(half) < NOPE
    for row, weights in ((16, key_up), (16 + half, value_up)):
        for j in range(heads // 2):
            upper = weights[0:half, j * LANES : (j + 1) * LANES].astype(f32)
            lower = weights[half:, j * LANES : (j + 1) * LANES].astype(f32)
            pair = (
                jnp.where(low_lane, upper, shifted(lower, NOPE)).astype(bf16),
                jnp.where(low_lane, shifted(upper, NOPE), lower).astype(bf16),
            )
            for n in (0, 1):
                for k in range(2 * j + n, kv, heads):
                    out[k, row : row + half, :] = pair[n]


def gathered_sum(first, out):
    total = first[0, 0:16, :].astype(f32)
    for k in range(1, first.shape[0]):
        total = total + first[k, 0:16, :].astype(f32)
    out[...] = total.astype(bf16)


def unpack(first, key_head, value_head):
    half = key_head.shape[0] // first.shape[0] // 2
    for k in range(first.shape[0]):
        for row, out in ((16, key_head), (16 + half, value_head)):
            tile = first[k, row : row + half, :]
            out[2 * half * k : 2 * half * k + half, :] = tile
            out[2 * half * k + half : 2 * half * (k + 1), :] = shifted(
                tile.astype(f32), NOPE
            ).astype(bf16)


def expand(own, r1, r2, r3, gains, query_up, key_gain, latent_gain, cosines, sines, out, rope_out, rope_tile, latent_out, *, width):
    kv, batch = out.shape[0], out.shape[1]
    rows = query_up.shape[0]
    low = (own[...].astype(f32) + r2[...].astype(f32)) + (
        r1[...].astype(f32) + r3[...].astype(f32)
    )
    lane = lane_of(batch)
    upper = low[0:8]
    inverse = lax.rsqrt(upper[:, rows : rows + 1] / width + epsilon)
    upper = upper * inverse
    query_low = jnp.where(lane < rows, upper, 0.0)
    squares = jnp.sum(query_low * query_low, axis=1, keepdims=True)
    own_gain = gains[pl.ds(lax.axis_index(KV), 1), :]
    part = dot((query_low * own_gain)[:, :rows].astype(bf16), query_up[...])
    size = NOPE + ROPE
    heads = part.shape[1] // size
    for n in range(heads):
        tile = jnp.where(
            lane < size, window(part, size * n, size), jnp.where(lane == size, squares, 0.0)
        ).astype(bf16)
        for k in range(n, kv, heads):
            out[k] = tile
    in_rope = (lane >= 2 * ROPE) & (lane < 3 * ROPE)
    rope = jnp.where(in_rope, upper, 0.0)
    rope = (
        rope
        * lax.rsqrt(jnp.sum(rope * rope, axis=1, keepdims=True) / ROPE + epsilon)
        * key_gain[...]
    )
    rope = shifted(rope * cosines[...] + swapped_halves(rope) * sines[...], -2 * ROPE)
    rope = jnp.where(lane < ROPE, rope, 0.0)
    rope_tile[...] = rope
    rope_out[...] = rope[:, :ROPE].astype(bf16)
    chosen = lax.broadcasted_iota(jnp.int32, inverse.shape, 0) == lax.axis_index("lo")
    latent = low[8:16] * jnp.sum(jnp.where(chosen, inverse, 0.0), axis=0, keepdims=True)
    mean = jnp.sum(jnp.sum(latent * latent, axis=1, keepdims=True), axis=0, keepdims=True) / (
        latent.shape[0] * latent.shape[1]
    )
    latent_out[...] = (latent * lax.rsqrt(mean + epsilon) * latent_gain[...]).astype(bf16)


def absorb(parts, key_head, gain, cosines, sines, latent, out, *, rank):
    total = parts[0].astype(f32)
    for k in range(1, parts.shape[0]):
        total = total + parts[k].astype(f32)
    lane = lane_of(total.shape[0])
    size = NOPE + ROPE
    queries = total * lax.rsqrt(total[:, size : size + 1] / rank + epsilon)
    squared = queries * queries
    nope = lane < NOPE
    in_rope = (lane >= NOPE) & (lane < size)
    mean_nope = jnp.sum(jnp.where(nope, squared, 0.0), axis=1, keepdims=True) / NOPE
    mean_rope = jnp.sum(jnp.where(in_rope, squared, 0.0), axis=1, keepdims=True) / ROPE
    queries = (
        queries
        * jnp.where(nope, lax.rsqrt(mean_nope + epsilon), lax.rsqrt(mean_rope + epsilon))
        * gain[...]
    )
    rope = queries * cosines[...] + swapped_halves(queries) * sines[...]
    rope = jnp.where(lane < ROPE, shifted(rope, -NOPE), 0.0).astype(bf16)
    own = lax.dot_general(
        jnp.where(nope, queries, 0.0).astype(bf16),
        key_head[...],
        (((1,), (1,)), ((), ())),
        preferred_element_type=f32,
    ).astype(bf16)
    columns = own.shape[1]
    for n in range(out.shape[0]):
        out[n, :, :columns] = own
        out[n, :, columns : columns + LANES] = rope
        out[n, :, columns + LANES :] = latent[...]


def attend(lengths, third, cache, ropes, new_rope, out, new_latent, by_batch):
    heads, batch = third.shape[0], third.shape[1]
    rank = cache.shape[2]
    context = cache.shape[1]
    rows = heads * batch
    kv_index = lax.axis_index(KV)
    queries = third[...].reshape(rows, third.shape[2])
    latent_q = queries[:, :rank]
    rope_q = queries[:, rank : rank + LANES]
    by_batch[...] = third[:, :, rank + LANES :].astype(f32)
    fresh_latent = jnp.concatenate([by_batch[:, j, :] for j in range(batch)], axis=1)
    new_latent[...] = fresh_latent.astype(bf16)
    tiled = jnp.concatenate([fresh_latent] * heads, axis=0)
    tiled_rope = jnp.concatenate([new_rope[...].astype(bf16).astype(f32)] * heads, axis=0)
    scale = (NOPE + ROPE) ** (-0.5)
    fresh = (
        jnp.sum(latent_q.astype(f32) * tiled, axis=1, keepdims=True)
        + jnp.sum(rope_q.astype(f32) * tiled_rope, axis=1, keepdims=True)
    ) * scale
    leader = kv_index == 0
    fresh = jnp.where(leader, fresh, lowest)
    of_row = lax.broadcasted_iota(jnp.int32, (rows, 1), 0) % batch
    scores = jnp.zeros((rows, context), f32)
    limit = jnp.zeros((rows, 1), jnp.int32)
    for b in range(batch):
        part = lax.dot_general(
            latent_q, cache[b], (((1,), (1,)), ((), ())), preferred_element_type=f32
        ) + dot(rope_q[:, :ROPE], ropes[b])
        scores = jnp.where(of_row == b, part, scores)
        limit = jnp.where(of_row == b, lengths[b], limit)
    positions = kv_index * context + lax.broadcasted_iota(jnp.int32, (rows, context), 1)
    usable = positions < limit
    masked = jnp.where(usable, scores * scale, lowest)
    top = jnp.maximum(jnp.max(masked, axis=1, keepdims=True), fresh)
    top_hi, top_lo = split_two(top)
    top = top_hi + top_lo
    weights = jnp.where(usable, jnp.exp(masked - top), 0.0)
    fresh_weight = jnp.where(leader, jnp.exp(fresh - top), 0.0)
    totals = jnp.sum(weights, axis=1, keepdims=True) + fresh_weight
    summed = fresh_weight.astype(bf16).astype(f32) * tiled
    for b in range(batch):
        own = jnp.where(of_row == b, weights, 0.0).astype(bf16)
        summed = summed + dot(own, cache[b])
    total_hi, total_lo = split_two(totals)
    lane = lane_of(rows)
    stats = jnp.where(
        lane == 0,
        top_hi,
        jnp.where(lane == 1, top_lo, jnp.where(lane == 2, total_hi, total_lo)),
    )
    out[:, :, :rank] = summed.astype(bf16).reshape(heads, batch, rank)
    out[:, :, rank:] = stats.astype(bf16).reshape(heads, batch, LANES)


def combine(fourth, value_head, out):
    sources, batch = fourth.shape[0], fourth.shape[1]
    rank = value_head.shape[0]
    stats = fourth[:, :, rank:].astype(f32)
    tops = stats[:, :, 0:1] + stats[:, :, 1:2]
    part_totals = stats[:, :, 2:3] + stats[:, :, 3:4]
    top_hi, top_lo = split_two(jnp.max(tops, axis=0))
    factors = jnp.exp(tops - (top_hi + top_lo)[None])
    totals = jnp.sum(part_totals * factors, axis=0)
    summed = factors[0] * fourth[0, :, :rank].astype(f32)
    for s in range(1, sources):
        summed = summed + factors[s] * fourth[s, :, :rank].astype(f32)
    latent_out = (summed / jnp.where(totals > 0.0, totals, 1.0)).astype(bf16)
    head = dot(latent_out, value_head[...])
    total_hi, total_lo = split_two(totals)
    lane = lane_of(batch)
    tile = jnp.where(
        lane < VDIM,
        head,
        jnp.where(
            lane == VDIM,
            top_hi,
            jnp.where(lane == VDIM + 1, top_lo, jnp.where(lane == VDIM + 2, total_hi, total_lo)),
        ),
    ).astype(bf16)
    for k in range(out.shape[0]):
        out[k] = tile


def project(fifth, output_proj, out):
    kv, batch = fifth.shape[0], fifth.shape[1]
    heads = output_proj.shape[0] // VDIM
    blocks = fifth[...].astype(f32).reshape(kv // heads, heads, batch, LANES)
    tops = blocks[..., VDIM : VDIM + 1] + blocks[..., VDIM + 1 : VDIM + 2]
    factors = jnp.exp(tops - jnp.max(tops, axis=0, keepdims=True)) * (
        blocks[..., VDIM + 2 : VDIM + 3] + blocks[..., VDIM + 3 : VDIM + 4]
    )
    heads_out = jnp.sum(blocks * factors, axis=0) / jnp.sum(factors, axis=0)
    low_lane = lane_of(batch) < VDIM
    tiles = [
        jnp.where(low_lane, heads_out[n], shifted(heads_out[n + 1], VDIM))
        for n in range(0, heads, 2)
    ]
    out[...] = dot(jnp.concatenate(tiles, axis=1).astype(bf16), output_proj[...]).astype(bf16)


def finish(own, r1, r2, r3, out):
    total = (own[...].astype(f32) + r2[...].astype(f32)) + (
        r1[...].astype(f32) + r3[...].astype(f32)
    )
    columns = out.shape[1]
    index = lax.axis_index("tp")
    result = total[:, :columns]
    for t in range(1, LANES // columns):
        result = jnp.where(index == t, shifted(total, -t * columns)[:, :columns], result)
    out[...] = result.astype(bf16)


def body(
    tokens,
    input_gain,
    query_down,
    latent_down,
    query_gain,
    query_up,
    nope_gain,
    query_rope_gain,
    key_up,
    latent_gain,
    key_rope_gain,
    latent_cache,
    rope_cache,
    lengths,
    value_up,
    output_proj,
):
    batch = tokens.shape[0]
    kv = lax.axis_size(KV)
    lo = lax.axis_size("lo")
    tp = lax.axis_size("tp")
    width = tokens.shape[1] * kv * tp
    heads = query_up.shape[1] // (NOPE + ROPE)
    own_rows = query_up.shape[0]
    q_rank = own_rows * kv
    kv_rank = latent_cache.shape[2]
    half = key_up.shape[0] // 2
    assert heads == lo == batch == 8 and kv_rank == 8 * LANES and tp == 4

    def shape(*dims, dtype=bf16):
        return jax.ShapeDtypeStruct(dims, dtype)

    lanes = jnp.arange(LANES)
    angles = lengths.astype(f32)[:, None] * theta ** (
        -(lanes % (ROPE // 2)).astype(f32) / (ROPE // 2)
    )
    cosines = jnp.cos(angles)
    sines = jnp.sin(angles) * jnp.where(lanes % ROPE < ROPE // 2, -1.0, 1.0)
    gains = jnp.pad(query_gain.reshape(kv, own_rows), ((0, 0), (0, LANES - own_rows)))
    head_gain = jnp.pad(jnp.concatenate([nope_gain, query_rope_gain]), (0, ROPE))[None]
    key_gain = jnp.pad(key_rope_gain, (2 * ROPE, ROPE))[None]

    first = exchange(
        run(
            compress,
            shape(kv, 16 + 2 * half, LANES),
            tokens,
            input_gain[None],
            query_down,
            latent_down,
            key_up,
            value_up,
            scratch=[pltpu.VMEM((batch, 8, LANES), f32)],
        ),
        KV,
    )
    low = run(gathered_sum, shape(16, LANES), first)
    others = from_others(low, "tp")
    key_head, value_head = run(unpack, (shape(kv_rank, LANES), shape(kv_rank, LANES)), first)

    second, new_rope_key, rope_tile, latent_row = run(
        lambda *refs: expand(*refs, width=width),
        (
            shape(kv, batch, LANES),
            shape(batch, ROPE),
            shape(batch, LANES, dtype=f32),
            shape(8, LANES),
        ),
        low,
        *others,
        gains,
        query_up,
        key_gain,
        latent_gain.reshape(8, LANES),
        cosines,
        sines,
    )
    second = exchange(second, KV)
    third = exchange(
        run(
            lambda *refs: absorb(*refs, rank=q_rank),
            shape(lo, batch, kv_rank + 2 * LANES),
            second,
            key_head,
            head_gain,
            cosines,
            sines,
            latent_row,
        ),
        "lo",
    )
    fourth, new_latent = run(
        attend,
        (shape(heads, batch, kv_rank + LANES), shape(batch, kv_rank)),
        lengths,
        third,
        latent_cache,
        rope_cache,
        rope_tile,
        scratch=[pltpu.VMEM((batch, 8, LANES), f32)],
        smem=(0,),
    )
    fourth = exchange(fourth, "lo")
    fifth = exchange(run(combine, shape(kv, batch, LANES), fourth, value_head), KV)
    partial = run(project, shape(batch, output_proj.shape[1]), fifth, output_proj)
    attended = run(
        finish, shape(batch, output_proj.shape[1] // tp), partial, *from_others(partial, "tp")
    )
    return (attended, new_latent, new_rope_key)


def solution(mesh):
    kv, lo = mesh.shape["kv"], 8
    split = Mesh(
        mesh.devices.reshape(mesh.shape["grp"], kv // lo, lo, mesh.shape["tp"]),
        ("grp", "hi", "lo", "tp"),
    )
    placed = (
        P("grp", KV_TP),
        P(KV_TP),
        P(KV_TP, None),
        P(KV_TP, None),
        P(),
        P(KV, "tp"),
        P(),
        P(),
        P(KV, "tp"),
        P(),
        P(),
        P("grp", KV, None),
        P("grp", None, KV),
        P("grp"),
        P(KV, "tp"),
        P("tp", KV),
    )
    return jax.shard_map(
        body,
        mesh=split,
        in_specs=placed,
        out_specs=(P("grp", KV_TP), P("grp", None), P("grp", None)),
        check_vma=False,
    )
```

time: 311 us -> 152 us (0.49)
  blocking collectives: 205 us -> 41.4 us
  Pallas kernels: 0 us -> 21.6 us
  matrix products: 12.6 us -> 0 us
  starting transfers between devices: 30 us -> 39.4 us
  other arithmetic: 8 us -> 2.64 us
  waiting for transfers between devices: 45.1 us -> 40.1 us
  local copies, waits for them, and re-layouts: 8.54 us -> 5.23 us
    psum x6 -> x0, blocking collectives: 168 us -> none  [one_axis_at_a_time(): return functools.reduce(lax.psum, axes, x)]
    pallas_call x0 -> x9, Pallas kernels: none -> 21.6 us  [run(): pl.pallas_call(kernel, out_shape=outs, in_specs=[IN_SMEM if i in smem els...]
    dot_general x11 -> x0, matrix products: 12.6 us -> none  [the longest x1 4.52 us: body(): jnp.einsum('bhr,bpr->bhp', query_latent, latent_cache, preferred_element_...]
    ppermute x0 -> x6, starting transfers between devices: none -> 9.87 us  [from_others(): lax.ppermute(x, axis, [(i, (i + s) % n) for i in range(n)])]
    all_to_all x5 -> x2, waiting for transfers between devices: 45.1 us -> 36.5 us  [exchange(): return lax.all_to_all(x, axes, 0, 0, tiled=True)]
    all_to_all x1 -> x3, blocking collectives: 37.1 us -> 41.4 us  [exchange(): return lax.all_to_all(x, axes, 0, 0, tiled=True)]
    ppermute x0 -> x6, waiting for transfers between devices: none -> 3.62 us  [from_others(): lax.ppermute(x, axis, [(i, (i + s) % n) for i in range(n)])]
    all_to_all x5 -> x2, starting transfers between devices: 30 us -> 29.5 us  [exchange(): return lax.all_to_all(x, axes, 0, 0, tiled=True)]
  transfers between devices with their start and end apart: 5 -> 8, of which waited for: 4 -> 5; matrix products, arithmetic and copies ran while one was open for 4% -> 4% of each run, Pallas kernels for 0% -> 1%
where the time goes in v1:
time: 152 us; the launch traced here: 151 us
  blocking collectives  41.4 us (27%)
  waiting for transfers between devices  40.1 us (26%)
  starting transfers between devices  39.4 us (26%)
  Pallas kernels  21.6 us (14%)
  local copies, waits for them, and re-layouts  5.23 us (3%)
  other arithmetic  2.64 us (2%)
    all_to_all x3, blocking collectives, exchange(): return lax.all_to_all(x, axes, 0, 0, tiled=True)  41.4 us
    all_to_all x2, waiting for transfers between devices, exchange(): return lax.all_to_all(x, axes, 0, 0, tiled=True)  36.5 us
    all_to_all x2, starting transfers between devices, exchange(): return lax.all_to_all(x, axes, 0, 0, tiled=True)  29.5 us
    pallas_call x9, Pallas kernels, run(): pl.pallas_call(kernel, out_shape=outs, in_specs=[IN_SMEM if i in smem els...  21.6 us
    ppermute x6, starting transfers between devices, from_others(): lax.ppermute(x, axis, [(i, (i + s) % n) for i in range(n)])  9.87 us
    ppermute x6, waiting for transfers between devices, from_others(): lax.ppermute(x, axis, [(i, (i + s) % n) for i in range(n)])  3.62 us
  transfers between devices with their start and end apart: 8, of which 5 were waited for; matrix products, arithmetic and copies ran while one was open for 4% of the time, Pallas kernels for 1%

profile of v1, /device:TPU:40, one launch (start us, length us, event | category | flops | bytes accessed | tf_op | source)
XLA Modules:
  0.0 151.0 jit_solution(9490491089840838140)
XLA Ops:
  0.6 2.0 %shard_map.175 = bf16[32,48,128]{2,1,0:T(8,128)(2,1)} custom-call(bf16[8,32]{1,0:T(8,128)(2,1)} %tokens.1, f32[1,32]{1,0:T(1,128)} %bitcast.7, bf16[32,1536]{1,0:T(8,128)(2,1)} %query_down.1, bf16[32,1056]{1,0:T(8,128)(2,1)} %latent_down.1, bf16[32,512]{1,0:T(8,128)(2,1)} %key_up.1, bf16[32,512]{1,0:T(8,128)(2,1)} %value_up.1), custom_call_target="tpu_custom_call" | custom-call | tf_op jit(solution)/shard_map/pallas_call | solution.py:28
  2.6 24.7 %all-to-all-start = ((bf16[32,48,128]{2,1,0:T(8,128)(2,1)}), bf16[32,48,128]{2,1,0:T(8,128)(2,1)S(1)}, u32[]{:S(2)}, u32[]{:S(2)}) async-start(bf16[32,48,128]{2,1,0:T(8,128)(2,1)} %shard_map.175), calls=%async_computation | async-start | bytes 786432 | tf_op jit(solution)/shard_map/all_to_all | solution.py:38
  27.3 0.7 convert_element_type.16
  28.0 0.7 fusion
  28.7 26.1 %all-to-all-done.first = bf16[32,48,128]{2,1,0:T(8,128)(2,1)S(1)} async-done(((bf16[32,48,128]{2,1,0:T(8,128)(2,1)}), bf16[32,48,128]{2,1,0:T(8,128)(2,1)S(1)}, u32[]{:S(2)}, u32[]{:S(2)}) %all-to-all-start) | async-done | bytes 393248 | tf_op jit(solution)/shard_map/all_to_all | solution.py:38
  54.9 0.8 copy-done
  55.6 1.6 %shard_map.176.refs_0_ = bf16[16,128]{1,0:T(8,128)(2,1)} custom-call(bf16[32,48,128]{2,1,0:T(8,128)(2,1)} %copy-done), custom_call_target="tpu_custom_call" | custom-call | tf_op jit(solution)/shard_map/pallas_call | solution.py:28
  57.2 1.6 %collective-permute-start = (bf16[16,128]{1,0:T(8,128)(2,1)}, bf16[16,128]{1,0:T(8,128)(2,1)S(1)}, u32[]{:S(2)}, u32[]{:S(2)}) collective-permute-start(bf16[16,128]{1,0:T(8,128)(2,1)} %shard_map.176.refs_0_), channel_id=1, source_target_pairs={{0,1},{1,2},{2,3},{3,0},{4,5},{5,6},{6,7},{7,4},{8,9},{9,10},{10,1... | collective-permute-start | bytes 12296 | tf_op jit(solution)/shard_map/ppermute | solution.py:43
  58.9 3.0 %collective-permute-start.1 = (bf16[16,128]{1,0:T(8,128)(2,1)}, bf16[16,128]{1,0:T(8,128)(2,1)S(1)}, u32[]{:S(2)}, u32[]{:S(2)}) collective-permute-start(bf16[16,128]{1,0:T(8,128)(2,1)} %shard_map.176.refs_0_), channel_id=1, source_target_pairs={{0,2},{1,3},{2,0},{3,1},{4,6},{5,7},{6,4},{7,5},{8,10},{9,11},{10,... | collective-permute-start | bytes 12296 | tf_op jit(solution)/shard_map/ppermute | solution.py:43
  61.9 1.3 collective-permute-start.2
  63.2 1.3 pad_bitcast_fusion.refs_6_
  64.5 0.8 reshape.37
  65.2 0.6 pad.12.refs_4_
  66.5 1.8 %shard_map.177 = (bf16[32,8,128]{2,1,0:T(8,128)(2,1)}, bf16[8,32]{1,0:T(8,128)(2,1)}, f32[8,128]{1,0:T(8,128)}, bf16[8,128]{1,0:T(8,128)(2,1)}) custom-call(bf16[16,128]{1,0:T(8,128)(2,1)} %shard_map.176.refs_0_, bf16[16,128]{1,0:T(8,128)(2,1)} %copy-done.2, bf16[16,128]{1,0:T(8,128)(2,1)} %copy-done.3, bf16[16,128]{1,0:T(8,128)(2,1)} %copy-done.4, ...), custom_call_target="tpu_custom_call" | custom-call | tf_op jit(solution)/shard_map/pallas_call | solution.py:28
  68.3 4.8 %all-to-all-start.1 = ((bf16[32,8,128]{2,1,0:T(8,128)(2,1)}), bf16[32,8,128]{2,1,0:T(8,128)(2,1)S(1)}, u32[]{:S(2)}, u32[]{:S(2)}) async-start(bf16[32,8,128]{2,1,0:T(8,128)(2,1)} %get-tuple-element.11), calls=%async_computation.1 | async-start | bytes 131072 | tf_op jit(solution)/shard_map/all_to_all | solution.py:38
  73.1 1.3 fusion.6.refs_2_
  74.3 2.0 %shard_map.178 = (bf16[1024,128]{1,0:T(8,128)(2,1)}, bf16[1024,128]{1,0:T(8,128)(2,1)}) custom-call(bf16[32,48,128]{2,1,0:T(8,128)(2,1)} %copy-done), custom_call_target="tpu_custom_call" | custom-call | tf_op jit(solution)/shard_map/pallas_call | solution.py:28
  76.3 10.4 %all-to-all-done.1.refs_0_ = bf16[32,8,128]{2,1,0:T(8,128)(2,1)S(1)} async-done(((bf16[32,8,128]{2,1,0:T(8,128)(2,1)}), bf16[32,8,128]{2,1,0:T(8,128)(2,1)S(1)}, u32[]{:S(2)}, u32[]{:S(2)}) %all-to-all-start.1) | async-done | bytes 65568 | tf_op jit(solution)/shard_map/all_to_all | solution.py:38
  86.7 0.6 copy-done.1
  87.3 2.0 %shard_map.179 = bf16[8,8,1280]{2,1,0:T(8,128)(2,1)} custom-call(bf16[32,8,128]{2,1,0:T(8,128)(2,1)} %copy-done.1, bf16[1024,128]{1,0:T(8,128)(2,1)} %get-tuple-element.12.refs_1_, f32[1,128]{1,0:T(1,128)} %fusion.6.refs_2_, f32[8,128]{1,0:T(8,128)} %get-tuple-element.20.refs_8_.refs_3_, f32[8,128]{1,0:T(8,128)} %get-tuple-element.19.refs_9_.refs_4_, ...), custom_call_target="tpu_custom_call" | custom-call | tf_op jit(solution)/shard_map/pallas_call | solution.py:28
  89.3 11.3 %all_to_all.25.third = bf16[8,8,1280]{2,1,0:T(8,128)(2,1)} all-to-all(bf16[8,8,1280]{2,1,0:T(8,128)(2,1)} %shard_map.179), channel_id=1, replica_groups=mesh['grp'=2,'hi'=4,'lo'=8,'tp'=4] {'lo'}, dimensions={0} | all-to-all | bytes 327680 | tf_op jit(solution)/shard_map/all_to_all | solution.py:38
  100.5 6.9 %shard_map.180 = (bf16[8,8,1152]{2,1,0:T(8,128)(2,1)}, bf16[8,1024]{1,0:T(8,128)(2,1)}) custom-call(s32[8]{0:T(128)} %lengths.1, bf16[8,8,1280]{2,1,0:T(8,128)(2,1)} %all_to_all.25.third, bf16[8,384,1024]{2,1,0:T(8,128)(2,1)} %cache.1, bf16[8,32,384]{2,1,0:T(8,128)(2,1)} %ropes.1, f32[8,128]{1,0:T(8,128)} %get-tuple-element.14.new_rope), custom_call_target="tpu_custom_call" | custom-call | tf_op jit(solution)/shard_map/pallas_call | solution.py:28
  107.5 11.1 %all_to_all.26.fourth = bf16[8,8,1152]{2,1,0:T(8,128)(2,1)} all-to-all(bf16[8,8,1152]{2,1,0:T(8,128)(2,1)} %get-tuple-element.15), channel_id=1, replica_groups=mesh['grp'=2,'hi'=4,'lo'=8,'tp'=4] {'lo'}, dimensions={0} | all-to-all | bytes 294912 | tf_op jit(solution)/shard_map/all_to_all | solution.py:38
  118.5 2.0 %shard_map.181 = bf16[32,8,128]{2,1,0:T(8,128)(2,1)} custom-call(bf16[8,8,1152]{2,1,0:T(8,128)(2,1)} %all_to_all.26.fourth, bf16[1024,128]{1,0:T(8,128)(2,1)} %get-tuple-element.16.value_head), custom_call_target="tpu_custom_call" | custom-call | tf_op jit(solution)/shard_map/pallas_call | solution.py:28
  120.6 19.0 %all_to_all.27.fifth = bf16[32,8,128]{2,1,0:T(8,128)(2,1)} all-to-all(bf16[32,8,128]{2,1,0:T(8,128)(2,1)} %shard_map.181), channel_id=1, replica_groups=mesh['grp'=2,'hi'=4,'lo'=8,'tp'=4] {'hi','lo'}, dimensions={0} | all-to-all | bytes 131072 | tf_op jit(solution)/shard_map/all_to_all | solution.py:38
  139.6 1.9 %shard_map.182.own = bf16[8,128]{1,0:T(8,128)(2,1)} custom-call(bf16[32,8,128]{2,1,0:T(8,128)(2,1)} %all_to_all.27.fifth, bf16[512,128]{1,0:T(8,128)(2,1)} %output_proj.1), custom_call_target="tpu_custom_call" | custom-call | tf_op jit(solution)/shard_map/pallas_call | solution.py:28
  141.5 0.7 collective-permute-start.3
  142.3 3.0 %collective-permute-start.4 = (bf16[8,128]{1,0:T(8,128)(2,1)}, bf16[8,128]{1,0:T(8,128)(2,1)S(1)}, u32[]{:S(2)}, u32[]{:S(2)}) collective-permute-start(bf16[8,128]{1,0:T(8,128)(2,1)} %shard_map.182.own), channel_id=1, source_target_pairs={{0,2},{1,3},{2,0},{3,1},{4,6},{5,7},{6,4},{7,5},{8,10},{9,11},{10,... | collective-permute-start | bytes 6152 | tf_op jit(solution)/shard_map/ppermute | solution.py:43
  145.5 1.1 collective-permute-done.3.r1
  146.5 1.0 collective-permute-done.4.r2
  147.6 1.5 %collective-permute-done.5.r3 = bf16[8,128]{1,0:T(8,128)(2,1)S(1)} collective-permute-done((bf16[8,128]{1,0:T(8,128)(2,1)}, bf16[8,128]{1,0:T(8,128)(2,1)S(1)}, u32[]{:S(2)}, u32[]{:S(2)}) %collective-permute-start.5) | collective-permute-done | bytes 2080 | tf_op jit(solution)/shard_map/ppermute | solution.py:43
  149.7 1.3 shard_map.183
  (19 shorter events, 1.3 us)
Async XLA Ops:
  2.6 52.3 %all-to-all-start = ((bf16[32,48,128]{2,1,0:T(8,128)(2,1)}), bf16[32,48,128]{2,1,0:T(8,128)(2,1)S(1)}, u32[]{:S(2)}, u32[]{:S(2)}) async-start(bf16[32,48,128]{2,1,0:T(8,128)(2,1)} %shard_map.175), calls=%async_computation | async-start | bytes 786432 | tf_op jit(solution)/shard_map/all_to_all | solution.py:38
  54.9 0.8 copy-start
  57.2 8.6 %collective-permute-start = (bf16[16,128]{1,0:T(8,128)(2,1)}, bf16[16,128]{1,0:T(8,128)(2,1)S(1)}, u32[]{:S(2)}, u32[]{:S(2)}) collective-permute-start(bf16[16,128]{1,0:T(8,128)(2,1)} %shard_map.176.refs_0_), channel_id=1, source_target_pairs={{0,1},{1,2},{2,3},{3,0},{4,5},{5,6},{6,7},{7,4},{8,9},{9,10},{10,1... | collective-permute-start | bytes 12296 | tf_op jit(solution)/shard_map/ppermute | solution.py:43
  58.9 7.0 %collective-permute-start.1 = (bf16[16,128]{1,0:T(8,128)(2,1)}, bf16[16,128]{1,0:T(8,128)(2,1)S(1)}, u32[]{:S(2)}, u32[]{:S(2)}) collective-permute-start(bf16[16,128]{1,0:T(8,128)(2,1)} %shard_map.176.refs_0_), channel_id=1, source_target_pairs={{0,2},{1,3},{2,0},{3,1},{4,6},{5,7},{6,4},{7,5},{8,10},{9,11},{10,... | collective-permute-start | bytes 12296 | tf_op jit(solution)/shard_map/ppermute | solution.py:43
  61.9 4.0 %collective-permute-start.2 = (bf16[16,128]{1,0:T(8,128)(2,1)}, bf16[16,128]{1,0:T(8,128)(2,1)S(1)}, u32[]{:S(2)}, u32[]{:S(2)}) collective-permute-start(bf16[16,128]{1,0:T(8,128)(2,1)} %shard_map.176.refs_0_), channel_id=1, source_target_pairs={{0,3},{1,0},{2,1},{3,2},{4,7},{5,4},{6,5},{7,6},{8,11},{9,8},{10,9... | collective-permute-start | bytes 12296 | tf_op jit(solution)/shard_map/ppermute | solution.py:43
  65.9 0.6 copy-start.2
  65.9 0.6 copy-start.3
  65.9 0.6 copy-start.4
  68.3 18.4 %all-to-all-start.1 = ((bf16[32,8,128]{2,1,0:T(8,128)(2,1)}), bf16[32,8,128]{2,1,0:T(8,128)(2,1)S(1)}, u32[]{:S(2)}, u32[]{:S(2)}) async-start(bf16[32,8,128]{2,1,0:T(8,128)(2,1)} %get-tuple-element.11), calls=%async_computation.1 | async-start | bytes 131072 | tf_op jit(solution)/shard_map/all_to_all | solution.py:38
  86.7 0.6 copy-start.1
  141.5 5.0 %collective-permute-start.3 = (bf16[8,128]{1,0:T(8,128)(2,1)}, bf16[8,128]{1,0:T(8,128)(2,1)S(1)}, u32[]{:S(2)}, u32[]{:S(2)}) collective-permute-start(bf16[8,128]{1,0:T(8,128)(2,1)} %shard_map.182.own), channel_id=1, source_target_pairs={{0,1},{1,2},{2,3},{3,0},{4,5},{5,6},{6,7},{7,4},{8,9},{9,10},{10,1... | collective-permute-start | bytes 6152 | tf_op jit(solution)/shard_map/ppermute | solution.py:43
  142.3 5.3 %collective-permute-start.4 = (bf16[8,128]{1,0:T(8,128)(2,1)}, bf16[8,128]{1,0:T(8,128)(2,1)S(1)}, u32[]{:S(2)}, u32[]{:S(2)}) collective-permute-start(bf16[8,128]{1,0:T(8,128)(2,1)} %shard_map.182.own), channel_id=1, source_target_pairs={{0,2},{1,3},{2,0},{3,1},{4,6},{5,7},{6,4},{7,5},{8,10},{9,11},{10,... | collective-permute-start | bytes 6152 | tf_op jit(solution)/shard_map/ppermute | solution.py:43
  145.3 3.8 %collective-permute-start.5 = (bf16[8,128]{1,0:T(8,128)(2,1)}, bf16[8,128]{1,0:T(8,128)(2,1)S(1)}, u32[]{:S(2)}, u32[]{:S(2)}) collective-permute-start(bf16[8,128]{1,0:T(8,128)(2,1)} %shard_map.182.own), channel_id=1, source_target_pairs={{0,3},{1,0},{2,1},{3,2},{4,7},{5,4},{6,5},{7,6},{8,11},{9,8},{10,9... | collective-permute-start | bytes 6152 | tf_op jit(solution)/shard_map/ppermute | solution.py:43
  146.5 2.6 %copy-start.5 = (bf16[8,128]{1,0:T(8,128)(2,1)}, bf16[8,128]{1,0:T(8,128)(2,1)S(1)}, u32[]{:S(2)}) copy-start(bf16[8,128]{1,0:T(8,128)(2,1)S(1)} %collective-permute-done.3.r1) | copy-start | bytes 6148
  147.6 1.5 %copy-start.6 = (bf16[8,128]{1,0:T(8,128)(2,1)}, bf16[8,128]{1,0:T(8,128)(2,1)S(1)}, u32[]{:S(2)}) copy-start(bf16[8,128]{1,0:T(8,128)(2,1)S(1)} %collective-permute-done.4.r2) | copy-start | bytes 6148
  149.1 0.6 copy-start.7

commit v2 on v1

--- a/solution.py
+++ b/solution.py
@@ -20,17 +20,21 @@
 f32 = jnp.float32
 bf16 = jnp.bfloat16
 
+FLOPS = 1 << 32
+VMEM_LIMIT = 16 << 20
 IN_VMEM = pl.BlockSpec(memory_space=pltpu.VMEM)
 IN_SMEM = pl.BlockSpec(memory_space=pltpu.SMEM)
 
 
-def run(kernel, outs, *args, scratch=(), smem=()):
+def run(kernel, outs, *args, scratch=(), smem=(), vmem=VMEM_LIMIT, flops=0):
     return pl.pallas_call(
         kernel,
         out_shape=outs,
         in_specs=[IN_SMEM if i in smem else IN_VMEM for i in range(len(args))],
         out_specs=jax.tree.map(lambda _: IN_VMEM, outs),
         scratch_shapes=scratch,
+        compiler_params=pltpu.CompilerParams(vmem_limit_bytes=vmem),
+        cost_estimate=pl.CostEstimate(flops=flops, transcendentals=0, bytes_accessed=0),
     )(*args)
 
 
@@ -109,7 +113,8 @@
                     out[k, row : row + half, :] = pair[n]
 
 
-def gathered_sum(first, out):
+def gathered_sum(first, *refs):
+    out = refs[-1]
     total = first[0, 0:16, :].astype(f32)
     for k in range(1, first.shape[0]):
         total = total + first[k, 0:16, :].astype(f32)
@@ -366,12 +371,13 @@
             key_up,
             value_up,
             scratch=[pltpu.VMEM((batch, 8, LANES), f32)],
+            vmem=60 << 20,
         ),
         KV,
     )
-    low = run(gathered_sum, shape(16, LANES), first)
+    low = run(gathered_sum, shape(16, LANES), first, cosines, sines, gains, head_gain, key_gain, flops=FLOPS)
     others = from_others(low, "tp")
-    key_head, value_head = run(unpack, (shape(kv_rank, LANES), shape(kv_rank, LANES)), first)
+    key_head, value_head = run(unpack, (shape(kv_rank, LANES), shape(kv_rank, LANES)), first, flops=FLOPS)
 
     second, new_rope_key, rope_tile, latent_row = run(
         lambda *refs: expand(*refs, width=width),
@@ -389,6 +395,7 @@
         latent_gain.reshape(8, LANES),
         cosines,
         sines,
+        flops=FLOPS,
     )
     second = exchange(second, KV)
     third = exchange(
@@ -401,6 +408,7 @@
             cosines,
             sines,
             latent_row,
+            flops=FLOPS,
         ),
         "lo",
     )

time: 152 us -> 134 us (0.88)
  Pallas kernels: 21.6 us -> 9.31 us
  waiting for transfers between devices: 40.1 us -> 45.9 us
  local copies, waits for them, and re-layouts: 5.23 us -> 0.81 us
  blocking collectives: 41.4 us -> 37.9 us
  starting transfers between devices: 39.4 us -> 37.5 us
    pallas_call x9, Pallas kernels: 21.6 us -> 9.31 us  [run(): pl.pallas_call(kernel, out_shape=outs, in_specs=[IN_SMEM if i in smem els...]
    ppermute x6, waiting for transfers between devices: 3.62 us -> 7.28 us  [from_others(): lax.ppermute(x, axis, [(i, (i + s) % n) for i in range(n)])]
    all_to_all x3, blocking collectives: 41.4 us -> 37.9 us  [exchange(): return lax.all_to_all(x, axes, 0, 0, tiled=True)]
    unnamed x16 -> x14, local copies, waits for them, and re-layouts: 2.54 us -> 0.03 us
    all_to_all x2, waiting for transfers between devices: 36.5 us -> 38.6 us  [exchange(): return lax.all_to_all(x, axes, 0, 0, tiled=True)]
    ppermute x6, starting transfers between devices: 9.87 us -> 8.04 us  [from_others(): lax.ppermute(x, axis, [(i, (i + s) % n) for i in range(n)])]
  transfers between devices with their start and end apart: 8 -> 8, of which waited for: 5 -> 7; matrix products, arithmetic and copies ran while one was open for 4% -> 2% of each run, Pallas kernels for 1% -> 0%
where the time goes in v2:
time: 134 us
  waiting for transfers between devices  45.9 us (34%)
  blocking collectives  37.9 us (28%)
  starting transfers between devices  37.5 us (28%)
  Pallas kernels  9.31 us (7%)
  other arithmetic  1.54 us (1%)
    all_to_all x2, waiting for transfers between devices, exchange(): return lax.all_to_all(x, axes, 0, 0, tiled=True)  38.6 us
    all_to_all x3, blocking collectives, exchange(): return lax.all_to_all(x, axes, 0, 0, tiled=True)  37.9 us
    all_to_all x2, starting transfers between devices, exchange(): return lax.all_to_all(x, axes, 0, 0, tiled=True)  29.5 us
    pallas_call x9, Pallas kernels, run(): pl.pallas_call(kernel, out_shape=outs, in_specs=[IN_SMEM if i in smem els...  9.31 us
    ppermute x6, starting transfers between devices, from_others(): lax.ppermute(x, axis, [(i, (i + s) % n) for i in range(n)])  8.04 us
    ppermute x6, waiting for transfers between devices, from_others(): lax.ppermute(x, axis, [(i, (i + s) % n) for i in range(n)])  7.28 us
  transfers between devices with their start and end apart: 8, of which 7 were waited for; matrix products, arithmetic and copies ran while one was open for 2% of the time, Pallas kernels for 0%

profile of v2, /device:TPU:40, one launch (start us, length us, event | category | flops | bytes accessed | tf_op | source)
XLA Modules:
  0.0 133.7 jit_solution(12712612574943344793)
XLA Ops:
  0.6 2.0 %shard_map.175 = bf16[32,48,128]{2,1,0:T(8,128)(2,1)} custom-call(bf16[8,32]{1,0:T(8,128)(2,1)} %tokens.1, f32[1,32]{1,0:T(1,128)} %bitcast.9, bf16[32,1536]{1,0:T(8,128)(2,1)} %query_down.1, bf16[32,1056]{1,0:T(8,128)(2,1)} %latent_down.1, bf16[32,512]{1,0:T(8,128)(2,1)} %key_up.1, bf16[32,512]{1,0:T(8,128)(2,1)} %value_up.1), custom_call_target="tpu_custom_call" | custom-call | tf_op jit(solution)/shard_map/pallas_call | solution.py:30
  2.6 24.7 %all-to-all-start = ((bf16[32,48,128]{2,1,0:T(8,128)(2,1)}), bf16[32,48,128]{2,1,0:T(8,128)(2,1)S(1)}, u32[]{:S(2)}, u32[]{:S(2)}) async-start(bf16[32,48,128]{2,1,0:T(8,128)(2,1)} %shard_map.175), calls=%async_computation | async-start | bytes 786432 | tf_op jit(solution)/shard_map/all_to_all | solution.py:42
  27.3 0.7 convert_element_type.16
  28.0 0.8 reshape.37
  28.8 0.8 pad_bitcast_fusion
  29.6 0.1 fusion
  29.7 25.2 %all-to-all-done.first = bf16[32,48,128]{2,1,0:T(8,128)(2,1)S(1)} async-done(((bf16[32,48,128]{2,1,0:T(8,128)(2,1)}), bf16[32,48,128]{2,1,0:T(8,128)(2,1)S(1)}, u32[]{:S(2)}, u32[]{:S(2)}) %all-to-all-start) | async-done | bytes 393248 | tf_op jit(solution)/shard_map/all_to_all | solution.py:42
  54.9 3.3 %collective-permute-start.2 = (bf16[16,128]{1,0:T(8,128)(2,1)S(1)}, bf16[16,128]{1,0:T(8,128)(2,1)S(1)}, u32[]{:S(2)}, u32[]{:S(2)}) collective-permute-start(bf16[16,128]{1,0:T(8,128)(2,1)S(1)} %shard_map.176.refs_0_), channel_id=1, source_target_pairs={{0,3},{1,0},{2,1},{3,2},{4,7},{5,4},{6,5},{7,6},{8,11},{9,8},{10,9... | collective-permute-start | bytes 12296 | tf_op jit(solution)/shard_map/ppermute | solution.py:47
  58.2 0.5 collective-permute-start.1
  58.7 1.0 collective-permute-start
  59.7 3.6 %collective-permute-done.1.refs_2_ = bf16[16,128]{1,0:T(8,128)(2,1)S(1)} collective-permute-done((bf16[16,128]{1,0:T(8,128)(2,1)S(1)}, bf16[16,128]{1,0:T(8,128)(2,1)S(1)}, u32[]{:S(2)}, u32[]{:S(2)}) %collective-permute-start.1) | collective-permute-done | bytes 4128 | tf_op jit(solution)/shard_map/ppermute | solution.py:47
  63.3 0.2 collective-permute-done.refs_1_
  63.5 0.9 shard_map.177
  64.4 4.7 %all-to-all-start.1 = ((bf16[32,8,128]{2,1,0:T(8,128)(2,1)}), bf16[32,8,128]{2,1,0:T(8,128)(2,1)S(1)}, u32[]{:S(2)}, u32[]{:S(2)}) async-start(bf16[32,8,128]{2,1,0:T(8,128)(2,1)} %get-tuple-element.11), calls=%async_computation.1 | async-start | bytes 131072 | tf_op jit(solution)/shard_map/all_to_all | solution.py:42
  69.2 0.0 slice-start
  69.2 0.2 shard_map.178
  69.4 13.4 %all-to-all-done.1.refs_0_ = bf16[32,8,128]{2,1,0:T(8,128)(2,1)S(1)} async-done(((bf16[32,8,128]{2,1,0:T(8,128)(2,1)}), bf16[32,8,128]{2,1,0:T(8,128)(2,1)S(1)}, u32[]{:S(2)}, u32[]{:S(2)}) %all-to-all-start.1) | async-done | bytes 65568 | tf_op jit(solution)/shard_map/all_to_all | solution.py:42
  82.8 0.3 shard_map.179
  83.1 0.0 copy-start.1
  83.1 10.0 %all_to_all.25.third = bf16[8,8,1280]{2,1,0:T(8,128)(2,1)S(1)} all-to-all(bf16[8,8,1280]{2,1,0:T(8,128)(2,1)S(1)} %shard_map.179), channel_id=1, replica_groups=mesh['grp'=2,'hi'=4,'lo'=8,'tp'=4] {'lo'}, dimensions={0} | all-to-all | bytes 327680 | tf_op jit(solution)/shard_map/all_to_all | solution.py:42
  93.1 4.5 %shard_map.180 = (bf16[8,8,1152]{2,1,0:T(8,128)(2,1)S(1)}, bf16[8,1024]{1,0:T(8,128)(2,1)}) custom-call(s32[8]{0:T(128)S(1)} %copy-done.2, bf16[8,8,1280]{2,1,0:T(8,128)(2,1)S(1)} %all_to_all.25.third, bf16[8,384,1024]{2,1,0:T(8,128)(2,1)S(1)} %bitcast.7, bf16[8,32,384]{2,1,0:T(8,128)(2,1)S(1)} %copy-done, f32[8,128]{1,0:T(8,128)S(1)} %get-tuple-element.14.new_rope), custom_call_target="tpu_custom_call" | custom-call | tf_op jit(solution)/shard_map/pallas_call | solution.py:30
  97.6 9.7 %all_to_all.26.fourth = bf16[8,8,1152]{2,1,0:T(8,128)(2,1)S(1)} all-to-all(bf16[8,8,1152]{2,1,0:T(8,128)(2,1)S(1)} %get-tuple-element.15), channel_id=1, replica_groups=mesh['grp'=2,'hi'=4,'lo'=8,'tp'=4] {'lo'}, dimensions={0} | all-to-all | bytes 294912 | tf_op jit(solution)/shard_map/all_to_all | solution.py:42
  107.3 0.4 shard_map.181
  107.6 18.2 %all_to_all.27.fifth = bf16[32,8,128]{2,1,0:T(8,128)(2,1)S(1)} all-to-all(bf16[32,8,128]{2,1,0:T(8,128)(2,1)S(1)} %shard_map.181), channel_id=1, replica_groups=mesh['grp'=2,'hi'=4,'lo'=8,'tp'=4] {'hi','lo'}, dimensions={0} | all-to-all | bytes 131072 | tf_op jit(solution)/shard_map/all_to_all | solution.py:42
  125.9 0.4 shard_map.182.own
  126.3 0.5 collective-permute-start.5
  126.8 1.4 %collective-permute-start.4 = (bf16[8,128]{1,0:T(8,128)(2,1)S(1)}, bf16[8,128]{1,0:T(8,128)(2,1)S(1)}, u32[]{:S(2)}, u32[]{:S(2)}) collective-permute-start(bf16[8,128]{1,0:T(8,128)(2,1)S(1)} %shard_map.182.own), channel_id=1, source_target_pairs={{0,2},{1,3},{2,0},{3,1},{4,6},{5,7},{6,4},{7,5},{8,10},{9,11},{10,... | collective-permute-start | bytes 6152 | tf_op jit(solution)/shard_map/ppermute | solution.py:47
  128.2 1.3 collective-permute-start.3
  129.5 0.4 collective-permute-done.5.r3
  129.9 2.0 %collective-permute-done.4.r2 = bf16[8,128]{1,0:T(8,128)(2,1)S(1)} collective-permute-done((bf16[8,128]{1,0:T(8,128)(2,1)S(1)}, bf16[8,128]{1,0:T(8,128)(2,1)S(1)}, u32[]{:S(2)}, u32[]{:S(2)}) %collective-permute-start.4) | collective-permute-done | bytes 2080 | tf_op jit(solution)/shard_map/ppermute | solution.py:47
  131.9 1.1 collective-permute-done.3.r1
  133.0 0.7 shard_map.183
  (17 shorter events, 0.1 us)
Async XLA Ops:
  2.6 52.3 %all-to-all-start = ((bf16[32,48,128]{2,1,0:T(8,128)(2,1)}), bf16[32,48,128]{2,1,0:T(8,128)(2,1)S(1)}, u32[]{:S(2)}, u32[]{:S(2)}) async-start(bf16[32,48,128]{2,1,0:T(8,128)(2,1)} %shard_map.175), calls=%async_computation | async-start | bytes 786432 | tf_op jit(solution)/shard_map/all_to_all | solution.py:42
  54.9 8.7 %copy-start.3 = (bf16[48,768]{1,0:T(8,128)(2,1)S(1)}, bf16[48,768]{1,0:T(8,128)(2,1)}, u32[]{:S(2)}) copy-start(bf16[48,768]{1,0:T(8,128)(2,1)} %refs_5_.1) | copy-start | bytes 221188
  54.9 8.7 %copy-start.4 = (f32[1024]{0:T(1024)S(1)}, f32[1024]{0:T(1024)}, u32[]{:S(2)}) copy-start(f32[1024]{0:T(1024)} %param.25) | copy-start | bytes 12292
  54.9 4.8 %collective-permute-start.2 = (bf16[16,128]{1,0:T(8,128)(2,1)S(1)}, bf16[16,128]{1,0:T(8,128)(2,1)S(1)}, u32[]{:S(2)}, u32[]{:S(2)}) collective-permute-start(bf16[16,128]{1,0:T(8,128)(2,1)S(1)} %shard_map.176.refs_0_), channel_id=1, source_target_pairs={{0,3},{1,0},{2,1},{3,2},{4,7},{5,4},{6,5},{7,6},{8,11},{9,8},{10,9... | collective-permute-start | bytes 12296 | tf_op jit(solution)/shard_map/ppermute | solution.py:47
  58.2 5.1 %collective-permute-start.1 = (bf16[16,128]{1,0:T(8,128)(2,1)S(1)}, bf16[16,128]{1,0:T(8,128)(2,1)S(1)}, u32[]{:S(2)}, u32[]{:S(2)}) collective-permute-start(bf16[16,128]{1,0:T(8,128)(2,1)S(1)} %shard_map.176.refs_0_), channel_id=1, source_target_pairs={{0,2},{1,3},{2,0},{3,1},{4,6},{5,7},{6,4},{7,5},{8,10},{9,11},{10,... | collective-permute-start | bytes 12296 | tf_op jit(solution)/shard_map/ppermute | solution.py:47
  58.7 4.8 %collective-permute-start = (bf16[16,128]{1,0:T(8,128)(2,1)S(1)}, bf16[16,128]{1,0:T(8,128)(2,1)S(1)}, u32[]{:S(2)}, u32[]{:S(2)}) collective-permute-start(bf16[16,128]{1,0:T(8,128)(2,1)S(1)} %shard_map.176.refs_0_), channel_id=1, source_target_pairs={{0,1},{1,2},{2,3},{3,0},{4,5},{5,6},{6,7},{7,4},{8,9},{9,10},{10,1... | collective-permute-start | bytes 12296 | tf_op jit(solution)/shard_map/ppermute | solution.py:47
  64.4 18.3 %all-to-all-start.1 = ((bf16[32,8,128]{2,1,0:T(8,128)(2,1)}), bf16[32,8,128]{2,1,0:T(8,128)(2,1)S(1)}, u32[]{:S(2)}, u32[]{:S(2)}) async-start(bf16[32,8,128]{2,1,0:T(8,128)(2,1)} %get-tuple-element.11), calls=%async_computation.1 | async-start | bytes 131072 | tf_op jit(solution)/shard_map/all_to_all | solution.py:42
  69.2 23.9 %slice-start = ((s8[6291456]{0:T(1024)(128)(4,1)}), s8[2097152]{0:T(1024)(128)(4,1)S(1)}, s32[]{:S(2)}) async-start(s8[6291456]{0:T(1024)(128)(4,1)} %bitcast.6), calls=%async_computation.5 | async-start | bytes 4194304
  82.8 10.3 %slice-start.1 = ((s8[6291456]{0:T(1024)(128)(4,1)}), s8[4194304]{0:T(1024)(128)(4,1)S(1)}, s32[]{:S(2)}) async-start(s8[6291456]{0:T(1024)(128)(4,1)} %bitcast.6), calls=%async_computation.6 | async-start | bytes 8388608
  82.8 10.3 %copy-start = (bf16[8,32,384]{2,1,0:T(8,128)(2,1)S(1)}, bf16[8,32,384]{2,1,0:T(8,128)(2,1)}, u32[]{:S(2)}) copy-start(bf16[8,32,384]{2,1,0:T(8,128)(2,1)} %ropes.1) | copy-start | bytes 589828
  82.8 10.3 %copy-start.2 = (s32[8]{0:T(128)S(1)}, s32[8]{0:T(128)}, u32[]{:S(2)}) copy-start(s32[8]{0:T(128)} %lengths.1) | copy-start | bytes 100
  83.1 42.7 %copy-start.1 = (bf16[512,128]{1,0:T(8,128)(2,1)S(1)}, bf16[512,128]{1,0:T(8,128)(2,1)}, u32[]{:S(2)}) copy-start(bf16[512,128]{1,0:T(8,128)(2,1)} %output_proj.1) | copy-start | bytes 393220
  126.3 3.6 %collective-permute-start.5 = (bf16[8,128]{1,0:T(8,128)(2,1)S(1)}, bf16[8,128]{1,0:T(8,128)(2,1)S(1)}, u32[]{:S(2)}, u32[]{:S(2)}) collective-permute-start(bf16[8,128]{1,0:T(8,128)(2,1)S(1)} %shard_map.182.own), channel_id=1, source_target_pairs={{0,3},{1,0},{2,1},{3,2},{4,7},{5,4},{6,5},{7,6},{8,11},{9,8},{10,9... | collective-permute-start | bytes 6152 | tf_op jit(solution)/shard_map/ppermute | solution.py:47
  126.8 5.1 %collective-permute-start.4 = (bf16[8,128]{1,0:T(8,128)(2,1)S(1)}, bf16[8,128]{1,0:T(8,128)(2,1)S(1)}, u32[]{:S(2)}, u32[]{:S(2)}) collective-permute-start(bf16[8,128]{1,0:T(8,128)(2,1)S(1)} %shard_map.182.own), channel_id=1, source_target_pairs={{0,2},{1,3},{2,0},{3,1},{4,6},{5,7},{6,4},{7,5},{8,10},{9,11},{10,... | collective-permute-start | bytes 6152 | tf_op jit(solution)/shard_map/ppermute | solution.py:47
  128.2 4.8 %collective-permute-start.3 = (bf16[8,128]{1,0:T(8,128)(2,1)S(1)}, bf16[8,128]{1,0:T(8,128)(2,1)S(1)}, u32[]{:S(2)}, u32[]{:S(2)}) collective-permute-start(bf16[8,128]{1,0:T(8,128)(2,1)S(1)} %shard_map.182.own), channel_id=1, source_target_pairs={{0,1},{1,2},{2,3},{3,0},{4,5},{5,6},{6,7},{7,4},{8,9},{9,10},{10,1... | collective-permute-start | bytes 6152 | tf_op jit(solution)/shard_map/ppermute | solution.py:47

commit v3 on v2

--- a/solution.py
+++ b/solution.py
@@ -10,6 +10,8 @@
 ROPE = 32
 VDIM = 64
 LANES = 128
+CUT = 32
+EDGE = 52
 KV = ("hi", "lo")
 KV_TP = ("hi", "lo", "tp")
 
@@ -42,11 +44,6 @@
     return lax.all_to_all(x, axes, 0, 0, tiled=True)
 
 
-def from_others(x, axis):
-    n = lax.axis_size(axis)
-    return [lax.ppermute(x, axis, [(i, (i + s) % n) for i in range(n)]) for s in range(1, n)]
-
-
 def lane_of(rows):
     return lax.broadcasted_iota(jnp.int32, (rows, LANES), 1)
 
@@ -82,7 +79,6 @@
     kv, batch = out.shape[0], tokens.shape[0]
     heads = by_batch.shape[0]
     own = query_down.shape[1] // kv
-    half = key_up.shape[0] // 2
     values = tokens[...].astype(f32)
     scaled = (values * gain[...]).astype(bf16)
     squares = jnp.sum(values * values, axis=1, keepdims=True)
@@ -91,16 +87,24 @@
     lane = lane_of(batch)
     rest = jnp.concatenate([part_l[:, 8 * LANES :], jnp.zeros((batch, LANES - ROPE), f32)], axis=1)
     fixed = jnp.where(lane < 2 * ROPE, squares, shifted(rest, 2 * ROPE))
-    for k in range(kv):
-        out[k, 0:8, :] = jnp.where(lane < own, window(part_q, own * k, own), fixed).astype(bf16)
     for j in range(8):
         by_batch[:, j, :] = part_l[:, j * LANES : (j + 1) * LANES]
     for n in range(heads):
-        tile = by_batch[n].astype(bf16)
+        latent = by_batch[n]
+        shared = fixed
+        for m in range(LANES // CUT):
+            shared = jnp.where(
+                lane == EDGE + m, shifted(latent, EDGE + m - (m * CUT + CUT - 1)), shared
+            )
         for k in range(n, kv, heads):
-            out[k, 8:16, :] = tile
+            tile = jnp.where(lane < own, window(part_q, own * k, own), shared)
+            tile = jnp.where(
+                lane < LANES - CUT, tile, shifted(latent, LANES - CUT - k // heads * CUT)
+            )
+            out[k, 0:8, :] = tile.astype(bf16)
+    half = key_up.shape[0] // 2
     low_lane = lane_of(half) < NOPE
-    for row, weights in ((16, key_up), (16 + half, value_up)):
+    for row, weights in ((8, key_up), (8 + half, value_up)):
         for j in range(heads // 2):
             upper = weights[0:half, j * LANES : (j + 1) * LANES].astype(f32)
             lower = weights[half:, j * LANES : (j + 1) * LANES].astype(f32)
@@ -113,18 +117,16 @@
                     out[k, row : row + half, :] = pair[n]
 
 
-def gathered_sum(first, *refs):
-    out = refs[-1]
-    total = first[0, 0:16, :].astype(f32)
+def gathered(first, *refs):
+    low, key_head, value_head = refs[-3:]
+    half = key_head.shape[0] // first.shape[0] // 2
+    total = first[0, 0:8, :].astype(f32)
     for k in range(1, first.shape[0]):
-        total = total + first[k, 0:16, :].astype(f32)
-    out[...] = total.astype(bf16)
-
-
-def unpack(first, key_head, value_head):
-    half = key_head.shape[0] // first.shape[0] // 2
+        total = total + first[k, 0:8, :].astype(f32)
+    for t in range(low.shape[0]):
+        low[t] = total.astype(bf16)
     for k in range(first.shape[0]):
-        for row, out in ((16, key_head), (16 + half, value_head)):
+        for row, out in ((8, key_head), (8 + half, value_head)):
             tile = first[k, row : row + half, :]
             out[2 * half * k : 2 * half * k + half, :] = tile
             out[2 * half * k + half : 2 * half * (k + 1), :] = shifted(
@@ -132,16 +134,26 @@
             ).astype(bf16)
 
 
-def expand(own, r1, r2, r3, gains, query_up, key_gain, latent_gain, cosines, sines, out, rope_out, rope_tile, latent_out, *, width):
+def total_of(parts):
+    total = parts[0].astype(f32)
+    for k in range(1, parts.shape[0]):
+        total = total + parts[k].astype(f32)
+    return total
+
+
+def expand(
+    parts, gains, query_up, key_gain, cosines, sines, out, rope_out, rope_tile, edges, *, width
+):
     kv, batch = out.shape[0], out.shape[1]
     rows = query_up.shape[0]
-    low = (own[...].astype(f32) + r2[...].astype(f32)) + (
-        r1[...].astype(f32) + r3[...].astype(f32)
-    )
+    low = total_of(parts)
     lane = lane_of(batch)
-    upper = low[0:8]
-    inverse = lax.rsqrt(upper[:, rows : rows + 1] / width + epsilon)
-    upper = upper * inverse
+    inverse = lax.rsqrt(low[:, rows : rows + 1] / width + epsilon)
+    upper = low * inverse
+    chosen = lax.broadcasted_iota(jnp.int32, inverse.shape, 0) == lax.axis_index("lo")
+    latent = low * jnp.sum(jnp.where(chosen, inverse, 0.0), axis=0, keepdims=True)
+    edges[...] = latent
+    latent = shifted(latent, 1)
     query_low = jnp.where(lane < rows, upper, 0.0)
     squares = jnp.sum(query_low * query_low, axis=1, keepdims=True)
     own_gain = gains[pl.ds(lax.axis_index(KV), 1), :]
@@ -150,7 +162,7 @@
     heads = part.shape[1] // size
     for n in range(heads):
         tile = jnp.where(
-            lane < size, window(part, size * n, size), jnp.where(lane == size, squares, 0.0)
+            lane < size, window(part, size * n, size), jnp.where(lane == size, squares, latent)
         ).astype(bf16)
         for k in range(n, kv, heads):
             out[k] = tile
@@ -165,18 +177,10 @@
     rope = jnp.where(lane < ROPE, rope, 0.0)
     rope_tile[...] = rope
     rope_out[...] = rope[:, :ROPE].astype(bf16)
-    chosen = lax.broadcasted_iota(jnp.int32, inverse.shape, 0) == lax.axis_index("lo")
-    latent = low[8:16] * jnp.sum(jnp.where(chosen, inverse, 0.0), axis=0, keepdims=True)
-    mean = jnp.sum(jnp.sum(latent * latent, axis=1, keepdims=True), axis=0, keepdims=True) / (
-        latent.shape[0] * latent.shape[1]
-    )
-    latent_out[...] = (latent * lax.rsqrt(mean + epsilon) * latent_gain[...]).astype(bf16)
-
-
-def absorb(parts, key_head, gain, cosines, sines, latent, out, *, rank):
-    total = parts[0].astype(f32)
-    for k in range(1, parts.shape[0]):
-        total = total + parts[k].astype(f32)
+
+
+def absorb(parts, key_head, gain, cosines, sines, edges, latent_gain, out, *, rank):
+    total = total_of(parts)
     lane = lane_of(total.shape[0])
     size = NOPE + ROPE
     queries = total * lax.rsqrt(total[:, size : size + 1] / rank + epsilon)
@@ -198,14 +202,26 @@
         (((1,), (1,)), ((), ())),
         preferred_element_type=f32,
     ).astype(bf16)
+    heads = out.shape[0]
+    latent = jnp.zeros_like(total)
+    for m in range(LANES // CUT):
+        piece = parts[m * heads + lax.axis_index("lo")].astype(f32)
+        here = (lane >= m * CUT) & (lane < m * CUT + CUT - 1)
+        latent = jnp.where(here, shifted(piece, m * CUT - size - 1), latent)
+        last = m * CUT + CUT - 1
+        latent = jnp.where(lane == last, shifted(edges[...], last - EDGE - m), latent)
+    mean = jnp.sum(jnp.sum(latent * latent, axis=1, keepdims=True), axis=0, keepdims=True) / (
+        latent.shape[0] * latent.shape[1]
+    )
+    latent = (latent * lax.rsqrt(mean + epsilon) * latent_gain[...]).astype(bf16)
     columns = own.shape[1]
     for n in range(out.shape[0]):
         out[n, :, :columns] = own
         out[n, :, columns : columns + LANES] = rope
-        out[n, :, columns + LANES :] = latent[...]
-
-
-def attend(lengths, third, cache, ropes, new_rope, out, new_latent, by_batch):
+        out[n, :, columns + LANES :] = latent
+
+
+def attend(lengths, third, cache, ropes, new_rope, out, new_latent, by_batch, all_scores, all_weights):
     heads, batch = third.shape[0], third.shape[1]
     rank = cache.shape[2]
     context = cache.shape[1]
@@ -227,14 +243,21 @@
     leader = kv_index == 0
     fresh = jnp.where(leader, fresh, lowest)
     of_row = lax.broadcasted_iota(jnp.int32, (rows, 1), 0) % batch
-    scores = jnp.zeros((rows, context), f32)
     limit = jnp.zeros((rows, 1), jnp.int32)
     for b in range(batch):
-        part = lax.dot_general(
-            latent_q, cache[b], (((1,), (1,)), ((), ())), preferred_element_type=f32
-        ) + dot(rope_q[:, :ROPE], ropes[b])
-        scores = jnp.where(of_row == b, part, scores)
         limit = jnp.where(of_row == b, lengths[b], limit)
+
+    @pl.when(kv_index >= 0)
+    def _():
+        scores = jnp.zeros((rows, context), f32)
+        for b in range(batch):
+            part = lax.dot_general(
+                latent_q, cache[b], (((1,), (1,)), ((), ())), preferred_element_type=f32
+            ) + dot(rope_q[:, :ROPE], ropes[b])
+            scores = jnp.where(of_row == b, part, scores)
+        all_scores[...] = scores
+
+    scores = all_scores[...]
     positions = kv_index * context + lax.broadcasted_iota(jnp.int32, (rows, context), 1)
     usable = positions < limit
     masked = jnp.where(usable, scores * scale, lowest)
@@ -244,10 +267,7 @@
     weights = jnp.where(usable, jnp.exp(masked - top), 0.0)
     fresh_weight = jnp.where(leader, jnp.exp(fresh - top), 0.0)
     totals = jnp.sum(weights, axis=1, keepdims=True) + fresh_weight
-    summed = fresh_weight.astype(bf16).astype(f32) * tiled
-    for b in range(batch):
-        own = jnp.where(of_row == b, weights, 0.0).astype(bf16)
-        summed = summed + dot(own, cache[b])
+    all_weights[...] = weights
     total_hi, total_lo = split_two(totals)
     lane = lane_of(rows)
     stats = jnp.where(
@@ -255,7 +275,15 @@
         top_hi,
         jnp.where(lane == 1, top_lo, jnp.where(lane == 2, total_hi, total_lo)),
     )
-    out[:, :, :rank] = summed.astype(bf16).reshape(heads, batch, rank)
+
+    @pl.when(kv_index >= 0)
+    def _():
+        summed = fresh_weight.astype(bf16).astype(f32) * tiled
+        for b in range(batch):
+            own = jnp.where(of_row == b, all_weights[...], 0.0).astype(bf16)
+            summed = summed + dot(own, cache[b])
+        out[:, :, :rank] = summed.astype(bf16).reshape(heads, batch, rank)
+
     out[:, :, rank:] = stats.astype(bf16).reshape(heads, batch, LANES)
 
 
@@ -302,13 +330,13 @@
         jnp.where(low_lane, heads_out[n], shifted(heads_out[n + 1], VDIM))
         for n in range(0, heads, 2)
     ]
-    out[...] = dot(jnp.concatenate(tiles, axis=1).astype(bf16), output_proj[...]).astype(bf16)
-
-
-def finish(own, r1, r2, r3, out):
-    total = (own[...].astype(f32) + r2[...].astype(f32)) + (
-        r1[...].astype(f32) + r3[...].astype(f32)
-    )
+    result = dot(jnp.concatenate(tiles, axis=1).astype(bf16), output_proj[...]).astype(bf16)
+    for t in range(out.shape[0]):
+        out[t] = result
+
+
+def finish(parts, out):
+    total = total_of(parts)
     columns = out.shape[1]
     index = lax.axis_index("tp")
     result = total[:, :columns]
@@ -363,7 +391,7 @@
     first = exchange(
         run(
             compress,
-            shape(kv, 16 + 2 * half, LANES),
+            shape(kv, batch + 2 * half, LANES),
             tokens,
             input_gain[None],
             query_down,
@@ -375,24 +403,31 @@
         ),
         KV,
     )
-    low = run(gathered_sum, shape(16, LANES), first, cosines, sines, gains, head_gain, key_gain, flops=FLOPS)
-    others = from_others(low, "tp")
-    key_head, value_head = run(unpack, (shape(kv_rank, LANES), shape(kv_rank, LANES)), first, flops=FLOPS)
-
-    second, new_rope_key, rope_tile, latent_row = run(
+    low, key_head, value_head = run(
+        gathered,
+        (shape(tp, batch, LANES), shape(kv_rank, LANES), shape(kv_rank, LANES)),
+        first,
+        cosines,
+        sines,
+        gains,
+        head_gain,
+        key_gain,
+        flops=FLOPS,
+    )
+    low = exchange(low, "tp")
+
+    second, new_rope_key, rope_tile, edges = run(
         lambda *refs: expand(*refs, width=width),
         (
             shape(kv, batch, LANES),
             shape(batch, ROPE),
             shape(batch, LANES, dtype=f32),
-            shape(8, LANES),
+            shape(batch, LANES, dtype=f32),
         ),
         low,
-        *others,
         gains,
         query_up,
         key_gain,
-        latent_gain.reshape(8, LANES),
         cosines,
         sines,
         flops=FLOPS,
@@ -407,7 +442,8 @@
             head_gain,
             cosines,
             sines,
-            latent_row,
+            edges,
+            latent_gain.reshape(8, LANES),
             flops=FLOPS,
         ),
         "lo",
@@ -420,15 +456,17 @@
         latent_cache,
         rope_cache,
         rope_tile,
-        scratch=[pltpu.VMEM((batch, 8, LANES), f32)],
+        scratch=[
+            pltpu.VMEM((batch, 8, LANES), f32),
+            pltpu.VMEM((heads * batch, latent_cache.shape[1]), f32),
+            pltpu.VMEM((heads * batch, latent_cache.shape[1]), f32),
+        ],
         smem=(0,),
     )
     fourth = exchange(fourth, "lo")
     fifth = exchange(run(combine, shape(kv, batch, LANES), fourth, value_head), KV)
-    partial = run(project, shape(batch, output_proj.shape[1]), fifth, output_proj)
-    attended = run(
-        finish, shape(batch, output_proj.shape[1] // tp), partial, *from_others(partial, "tp")
-    )
+    partial = run(project, shape(tp, batch, output_proj.shape[1]), fifth, output_proj)
+    attended = run(finish, shape(batch, output_proj.shape[1] // tp), exchange(partial, "tp"))
     return (attended, new_latent, new_rope_key)
 
 

time: 134 us -> 133 us (level)
  blocking collectives: 37.9 us -> 72.7 us
  waiting for transfers between devices: 45.9 us -> 22.4 us
  starting transfers between devices: 37.5 us -> 24.7 us
    all_to_all x3 -> x6, blocking collectives: 37.9 us -> 72.7 us  [exchange(): return lax.all_to_all(x, axes, 0, 0, tiled=True)]
    all_to_all x2 -> x1, waiting for transfers between devices: 38.6 us -> 22.4 us  [exchange(): return lax.all_to_all(x, axes, 0, 0, tiled=True)]
    ppermute x6 -> x0, starting transfers between devices: 8.04 us -> none  [from_others(): lax.ppermute(x, axis, [(i, (i + s) % n) for i in range(n)])]
    ppermute x6 -> x0, waiting for transfers between devices: 7.28 us -> none  [from_others(): lax.ppermute(x, axis, [(i, (i + s) % n) for i in range(n)])]
    all_to_all x2 -> x1, starting transfers between devices: 29.5 us -> 24.7 us  [exchange(): return lax.all_to_all(x, axes, 0, 0, tiled=True)]
    pallas_call x9 -> x8, Pallas kernels: 9.31 us -> 9.67 us  [run(): pl.pallas_call(kernel, out_shape=outs, in_specs=[IN_SMEM if i in smem els...]
  transfers between devices with their start and end apart: 8 -> 1, of which waited for: 7 -> 1; matrix products, arithmetic and copies ran while one was open for 2% -> 2% of each run, Pallas kernels for 0% -> 0%
where the time goes in v3:
time: 133 us
  blocking collectives  72.7 us (55%)
  starting transfers between devices  24.7 us (19%)
  waiting for transfers between devices  22.4 us (17%)
  Pallas kernels  9.67 us (7%)
  other arithmetic  1.54 us (1%)
    all_to_all x6, blocking collectives, exchange(): return lax.all_to_all(x, axes, 0, 0, tiled=True)  72.7 us
    all_to_all x1, starting transfers between devices, exchange(): return lax.all_to_all(x, axes, 0, 0, tiled=True)  24.7 us
    all_to_all x1, waiting for transfers between devices, exchange(): return lax.all_to_all(x, axes, 0, 0, tiled=True)  22.4 us
    pallas_call x8, Pallas kernels, run(): pl.pallas_call(kernel, out_shape=outs, in_specs=[IN_SMEM if i in smem els...  9.67 us
  transfers between devices with their start and end apart: 1, of which 1 were waited for; matrix products, arithmetic and copies ran while one was open for 2% of the time, Pallas kernels for 0%

profile of v3, /device:TPU:40, one launch (start us, length us, event | category | flops | bytes accessed | tf_op | source)
XLA Modules:
  0.0 132.6 jit_solution(12282495722603072512)
XLA Ops:
  0.6 2.0 %shard_map.175 = bf16[32,40,128]{2,1,0:T(8,128)(2,1)} custom-call(bf16[8,32]{1,0:T(8,128)(2,1)} %tokens.1, f32[1,32]{1,0:T(1,128)} %bitcast.9, bf16[32,1536]{1,0:T(8,128)(2,1)} %query_down.1, bf16[32,1056]{1,0:T(8,128)(2,1)} %latent_down.1, bf16[32,512]{1,0:T(8,128)(2,1)} %key_up.1, bf16[32,512]{1,0:T(8,128)(2,1)} %value_up.1), custom_call_target="tpu_custom_call" | custom-call | tf_op jit(solution)/shard_map/pallas_call | solution.py:32
  2.6 24.7 %all-to-all-start = ((bf16[32,40,128]{2,1,0:T(8,128)(2,1)}), bf16[32,40,128]{2,1,0:T(8,128)(2,1)S(1)}, u32[]{:S(2)}, u32[]{:S(2)}) async-start(bf16[32,40,128]{2,1,0:T(8,128)(2,1)} %shard_map.175), calls=%async_computation | async-start | bytes 655360 | tf_op jit(solution)/shard_map/all_to_all | solution.py:44
  27.4 0.7 convert_element_type.16
  28.0 0.8 reshape.37
  28.8 0.8 pad_bitcast_fusion
  29.6 0.1 fusion
  29.7 22.4 %all-to-all-done.first = bf16[32,40,128]{2,1,0:T(8,128)(2,1)S(1)} async-done(((bf16[32,40,128]{2,1,0:T(8,128)(2,1)}), bf16[32,40,128]{2,1,0:T(8,128)(2,1)S(1)}, u32[]{:S(2)}, u32[]{:S(2)}) %all-to-all-start) | async-done | bytes 327712 | tf_op jit(solution)/shard_map/all_to_all | solution.py:44
  52.1 0.0 copy-start.3
  52.1 0.2 shard_map.176
  52.3 9.7 %all_to_all.35.refs_0_ = bf16[4,8,128]{2,1,0:T(8,128)(2,1)S(1)} all-to-all(bf16[4,8,128]{2,1,0:T(8,128)(2,1)S(1)} %get-tuple-element.12), channel_id=1, replica_groups=mesh['grp'=2,'hi'=4,'lo'=8,'tp'=4] {'tp'}, dimensions={0} | all-to-all | bytes 16384 | tf_op jit(solution)/shard_map/all_to_all | solution.py:44
  62.0 0.0 copy-done.3
  62.0 0.0 copy-start.4
  62.0 0.0 slice-start
  62.0 0.9 shard_map.177
  62.9 17.6 %all_to_all.36.refs_0_ = bf16[32,8,128]{2,1,0:T(8,128)(2,1)S(1)} all-to-all(bf16[32,8,128]{2,1,0:T(8,128)(2,1)S(1)} %get-tuple-element.13), channel_id=1, replica_groups=mesh['grp'=2,'hi'=4,'lo'=8,'tp'=4] {'hi','lo'}, dimensions={0} | all-to-all | bytes 131072 | tf_op jit(solution)/shard_map/all_to_all | solution.py:44
  80.5 0.0 copy-done.4
  80.5 0.0 slice-start.1
  80.5 0.3 shard_map.178
  80.9 0.0 copy-start.1
  80.9 9.8 %all_to_all.37.third = bf16[8,8,1280]{2,1,0:T(8,128)(2,1)S(1)} all-to-all(bf16[8,8,1280]{2,1,0:T(8,128)(2,1)S(1)} %shard_map.178), channel_id=1, replica_groups=mesh['grp'=2,'hi'=4,'lo'=8,'tp'=4] {'lo'}, dimensions={0} | all-to-all | bytes 327680 | tf_op jit(solution)/shard_map/all_to_all | solution.py:44
  90.7 0.0 slice-done
  90.7 0.0 slice-done.1
  90.7 0.0 copy-done
  90.7 0.0 copy-done.2
  90.7 4.8 %shard_map.179 = (bf16[8,8,1152]{2,1,0:T(8,128)(2,1)S(1)}, bf16[8,1024]{1,0:T(8,128)(2,1)}) custom-call(s32[8]{0:T(128)S(1)} %copy-done.2, bf16[8,8,1280]{2,1,0:T(8,128)(2,1)S(1)} %all_to_all.37.third, bf16[8,384,1024]{2,1,0:T(8,128)(2,1)S(1)} %bitcast.7, bf16[8,32,384]{2,1,0:T(8,128)(2,1)S(1)} %copy-done, f32[8,128]{1,0:T(8,128)S(1)} %get-tuple-element.16.new_rope), custom_call_target="tpu_custom_call" | custom-call | tf_op jit(solution)/shard_map/pallas_call | solution.py:32
  95.6 9.7 %all_to_all.38.fourth = bf16[8,8,1152]{2,1,0:T(8,128)(2,1)S(1)} all-to-all(bf16[8,8,1152]{2,1,0:T(8,128)(2,1)S(1)} %get-tuple-element.17), channel_id=1, replica_groups=mesh['grp'=2,'hi'=4,'lo'=8,'tp'=4] {'lo'}, dimensions={0} | all-to-all | bytes 294912 | tf_op jit(solution)/shard_map/all_to_all | solution.py:44
  105.2 0.4 shard_map.180
  105.6 18.3 %all_to_all.39.fifth = bf16[32,8,128]{2,1,0:T(8,128)(2,1)S(1)} all-to-all(bf16[32,8,128]{2,1,0:T(8,128)(2,1)S(1)} %shard_map.180), channel_id=1, replica_groups=mesh['grp'=2,'hi'=4,'lo'=8,'tp'=4] {'hi','lo'}, dimensions={0} | all-to-all | bytes 131072 | tf_op jit(solution)/shard_map/all_to_all | solution.py:44
  123.9 0.0 copy-done.1
  123.9 0.4 shard_map.181
  124.3 7.7 %all_to_all.40.parts = bf16[4,8,128]{2,1,0:T(8,128)(2,1)S(1)} all-to-all(bf16[4,8,128]{2,1,0:T(8,128)(2,1)S(1)} %shard_map.181), channel_id=1, replica_groups=mesh['grp'=2,'hi'=4,'lo'=8,'tp'=4] {'tp'}, dimensions={0} | all-to-all | bytes 16384 | tf_op jit(solution)/shard_map/all_to_all | solution.py:44
  132.0 0.7 shard_map.182
  (5 shorter events, 0.0 us)
Async XLA Ops:
  2.6 49.5 %all-to-all-start = ((bf16[32,40,128]{2,1,0:T(8,128)(2,1)}), bf16[32,40,128]{2,1,0:T(8,128)(2,1)S(1)}, u32[]{:S(2)}, u32[]{:S(2)}) async-start(bf16[32,40,128]{2,1,0:T(8,128)(2,1)} %shard_map.175), calls=%async_computation | async-start | bytes 655360 | tf_op jit(solution)/shard_map/all_to_all | solution.py:44
  52.1 9.9 %copy-start.3 = (bf16[48,768]{1,0:T(8,128)(2,1)S(1)}, bf16[48,768]{1,0:T(8,128)(2,1)}, u32[]{:S(2)}) copy-start(bf16[48,768]{1,0:T(8,128)(2,1)} %refs_2_.1) | copy-start | bytes 221188
  62.0 18.5 %copy-start.4 = (f32[1024]{0:T(1024)S(1)}, f32[1024]{0:T(1024)}, u32[]{:S(2)}) copy-start(f32[1024]{0:T(1024)} %param.25) | copy-start | bytes 12292
  62.0 28.7 %slice-start = ((s8[6291456]{0:T(1024)(128)(4,1)}), s8[4194304]{0:T(1024)(128)(4,1)S(1)}, s32[]{:S(2)}) async-start(s8[6291456]{0:T(1024)(128)(4,1)} %bitcast.6), calls=%async_computation.7 | async-start | bytes 8388608
  80.5 10.2 %slice-start.1 = ((s8[6291456]{0:T(1024)(128)(4,1)}), s8[2097152]{0:T(1024)(128)(4,1)S(1)}, s32[]{:S(2)}) async-start(s8[6291456]{0:T(1024)(128)(4,1)} %bitcast.6), calls=%async_computation.8 | async-start | bytes 4194304
  80.5 10.2 %copy-start = (bf16[8,32,384]{2,1,0:T(8,128)(2,1)S(1)}, bf16[8,32,384]{2,1,0:T(8,128)(2,1)}, u32[]{:S(2)}) copy-start(bf16[8,32,384]{2,1,0:T(8,128)(2,1)} %ropes.1) | copy-start | bytes 589828
  80.5 10.2 %copy-start.2 = (s32[8]{0:T(128)S(1)}, s32[8]{0:T(128)}, u32[]{:S(2)}) copy-start(s32[8]{0:T(128)} %lengths.1) | copy-start | bytes 100
  80.9 43.0 %copy-start.1 = (bf16[512,128]{1,0:T(8,128)(2,1)S(1)}, bf16[512,128]{1,0:T(8,128)(2,1)}, u32[]{:S(2)}) copy-start(bf16[512,128]{1,0:T(8,128)(2,1)} %output_proj.1) | copy-start | bytes 393220

commit v4 on v3

--- a/solution.py
+++ b/solution.py
@@ -142,7 +142,7 @@
 
 
 def expand(
-    parts, gains, query_up, key_gain, cosines, sines, out, rope_out, rope_tile, edges, *, width
+    parts, gains, query_up, key_gain, cosines, sines, out, rope_tile, edges, *, width
 ):
     kv, batch = out.shape[0], out.shape[1]
     rows = query_up.shape[0]
@@ -175,8 +175,7 @@
     )
     rope = shifted(rope * cosines[...] + swapped_halves(rope) * sines[...], -2 * ROPE)
     rope = jnp.where(lane < ROPE, rope, 0.0)
-    rope_tile[...] = rope
-    rope_out[...] = rope[:, :ROPE].astype(bf16)
+    rope_tile[...] = rope.astype(bf16).astype(f32)
 
 
 def absorb(parts, key_head, gain, cosines, sines, edges, latent_gain, out, *, rank):
@@ -221,70 +220,55 @@
         out[n, :, columns + LANES :] = latent
 
 
-def attend(lengths, third, cache, ropes, new_rope, out, new_latent, by_batch, all_scores, all_weights):
+def soften(
+    lengths, third, products, ropes, new_rope, weights_out, fresh_out, stats_out, new_latent, wide, tail
+):
     heads, batch = third.shape[0], third.shape[1]
-    rank = cache.shape[2]
-    context = cache.shape[1]
-    rows = heads * batch
+    rank = new_latent.shape[1]
+    context = products.shape[2]
     kv_index = lax.axis_index(KV)
-    queries = third[...].reshape(rows, third.shape[2])
-    latent_q = queries[:, :rank]
-    rope_q = queries[:, rank : rank + LANES]
-    by_batch[...] = third[:, :, rank + LANES :].astype(f32)
-    fresh_latent = jnp.concatenate([by_batch[:, j, :] for j in range(batch)], axis=1)
-    new_latent[...] = fresh_latent.astype(bf16)
-    tiled = jnp.concatenate([fresh_latent] * heads, axis=0)
-    tiled_rope = jnp.concatenate([new_rope[...].astype(bf16).astype(f32)] * heads, axis=0)
+    leader = kv_index == 0
     scale = (NOPE + ROPE) ** (-0.5)
-    fresh = (
-        jnp.sum(latent_q.astype(f32) * tiled, axis=1, keepdims=True)
-        + jnp.sum(rope_q.astype(f32) * tiled_rope, axis=1, keepdims=True)
-    ) * scale
-    leader = kv_index == 0
-    fresh = jnp.where(leader, fresh, lowest)
-    of_row = lax.broadcasted_iota(jnp.int32, (rows, 1), 0) % batch
-    limit = jnp.zeros((rows, 1), jnp.int32)
+    wide[...] = third[:, :, : rank + LANES].astype(f32)
+    tail[...] = third[:, :, rank + LANES :].astype(f32)
+    latent = jnp.concatenate([tail[:, j, :] for j in range(rank // LANES)], axis=1)
+    new_latent[...] = latent.astype(bf16)
+    positions = kv_index * context + lax.broadcasted_iota(jnp.int32, (heads, context), 1)
+    lane = lane_of(heads)
     for b in range(batch):
-        limit = jnp.where(of_row == b, lengths[b], limit)
-
-    @pl.when(kv_index >= 0)
-    def _():
-        scores = jnp.zeros((rows, context), f32)
-        for b in range(batch):
-            part = lax.dot_general(
-                latent_q, cache[b], (((1,), (1,)), ((), ())), preferred_element_type=f32
-            ) + dot(rope_q[:, :ROPE], ropes[b])
-            scores = jnp.where(of_row == b, part, scores)
-        all_scores[...] = scores
-
-    scores = all_scores[...]
-    positions = kv_index * context + lax.broadcasted_iota(jnp.int32, (rows, context), 1)
-    usable = positions < limit
-    masked = jnp.where(usable, scores * scale, lowest)
-    top = jnp.maximum(jnp.max(masked, axis=1, keepdims=True), fresh)
-    top_hi, top_lo = split_two(top)
-    top = top_hi + top_lo
-    weights = jnp.where(usable, jnp.exp(masked - top), 0.0)
-    fresh_weight = jnp.where(leader, jnp.exp(fresh - top), 0.0)
-    totals = jnp.sum(weights, axis=1, keepdims=True) + fresh_weight
-    all_weights[...] = weights
-    total_hi, total_lo = split_two(totals)
-    lane = lane_of(rows)
-    stats = jnp.where(
-        lane == 0,
-        top_hi,
-        jnp.where(lane == 1, top_lo, jnp.where(lane == 2, total_hi, total_lo)),
-    )
-
-    @pl.when(kv_index >= 0)
-    def _():
-        summed = fresh_weight.astype(bf16).astype(f32) * tiled
-        for b in range(batch):
-            own = jnp.where(of_row == b, all_weights[...], 0.0).astype(bf16)
-            summed = summed + dot(own, cache[b])
-        out[:, :, :rank] = summed.astype(bf16).reshape(heads, batch, rank)
-
-    out[:, :, rank:] = stats.astype(bf16).reshape(heads, batch, LANES)
+        query = wide[:, b, :]
+        rope = query[:, rank:]
+        scores = products[b] + dot(rope[:, :ROPE].astype(bf16), ropes[b])
+        fresh = (
+            jnp.sum(query[:, :rank] * latent[b : b + 1], axis=1, keepdims=True)
+            + jnp.sum(rope * new_rope[b : b + 1, :], axis=1, keepdims=True)
+        ) * scale
+        fresh = jnp.where(leader, fresh, lowest)
+        usable = positions < lengths[b]
+        masked = jnp.where(usable, scores * scale, lowest)
+        top_hi, top_lo = split_two(
+            jnp.maximum(jnp.max(masked, axis=1, keepdims=True), fresh)
+        )
+        top = top_hi + top_lo
+        weights = jnp.where(usable, jnp.exp(masked - top), 0.0)
+        fresh_weight = jnp.where(leader, jnp.exp(fresh - top), 0.0)
+        total_hi, total_lo = split_two(jnp.sum(weights, axis=1, keepdims=True) + fresh_weight)
+        weights_out[b] = weights.astype(bf16)
+        fresh_out[b] = jnp.broadcast_to(fresh_weight.astype(bf16).astype(f32), (heads, LANES))
+        stats_out[:, b, :] = jnp.where(
+            lane == 0,
+            top_hi,
+            jnp.where(lane == 1, top_lo, jnp.where(lane == 2, total_hi, total_lo)),
+        )
+
+
+def assemble(summed, fresh, stats, new_latent, out, wide):
+    batch, heads, rank = summed.shape
+    for b in range(batch):
+        latent = new_latent[...].astype(f32)[b : b + 1]
+        wide[:, b, :] = summed[b] + fresh[b][:, 0:1] * latent
+    out[:, :, :rank] = wide[...].astype(bf16)
+    out[:, :, rank:] = stats[...].astype(bf16)
 
 
 def combine(fourth, value_head, out):
@@ -335,7 +319,9 @@
         out[t] = result
 
 
-def finish(parts, out):
+def finish(parts, latent, rope, out, latent_out, rope_out):
+    latent_out[...] = latent[...]
+    rope_out[...] = rope[:, : rope_out.shape[1]].astype(bf16)
     total = total_of(parts)
     columns = out.shape[1]
     index = lax.axis_index("tp")
@@ -416,11 +402,10 @@
     )
     low = exchange(low, "tp")
 
-    second, new_rope_key, rope_tile, edges = run(
+    second, rope_tile, edges = run(
         lambda *refs: expand(*refs, width=width),
         (
             shape(kv, batch, LANES),
-            shape(batch, ROPE),
             shape(batch, LANES, dtype=f32),
             shape(batch, LANES, dtype=f32),
         ),
@@ -448,26 +433,49 @@
         ),
         "lo",
     )
-    fourth, new_latent = run(
-        attend,
-        (shape(heads, batch, kv_rank + LANES), shape(batch, kv_rank)),
+    products = jnp.einsum(
+        "hbr,bpr->bhp", third[:, :, :kv_rank], latent_cache, preferred_element_type=f32
+    )
+    context = latent_cache.shape[1]
+    weights, fresh, stats, new_latent = run(
+        soften,
+        (
+            shape(batch, heads, context),
+            shape(batch, heads, LANES, dtype=f32),
+            shape(heads, batch, LANES, dtype=f32),
+            shape(batch, kv_rank),
+        ),
         lengths,
         third,
-        latent_cache,
+        products,
         rope_cache,
         rope_tile,
         scratch=[
+            pltpu.VMEM((heads, batch, kv_rank + LANES), f32),
             pltpu.VMEM((batch, 8, LANES), f32),
-            pltpu.VMEM((heads * batch, latent_cache.shape[1]), f32),
-            pltpu.VMEM((heads * batch, latent_cache.shape[1]), f32),
         ],
         smem=(0,),
+    )
+    summed = jnp.einsum("bhp,bpr->bhr", weights, latent_cache, preferred_element_type=f32)
+    fourth = run(
+        assemble,
+        shape(heads, batch, kv_rank + LANES),
+        summed,
+        fresh,
+        stats,
+        new_latent,
+        scratch=[pltpu.VMEM((heads, batch, kv_rank), f32)],
     )
     fourth = exchange(fourth, "lo")
     fifth = exchange(run(combine, shape(kv, batch, LANES), fourth, value_head), KV)
     partial = run(project, shape(tp, batch, output_proj.shape[1]), fifth, output_proj)
-    attended = run(finish, shape(batch, output_proj.shape[1] // tp), exchange(partial, "tp"))
-    return (attended, new_latent, new_rope_key)
+    return run(
+        finish,
+        (shape(batch, output_proj.shape[1] // tp), shape(batch, kv_rank), shape(batch, ROPE)),
+        exchange(partial, "tp"),
+        new_latent,
+        rope_tile,
+    )
 
 
 def solution(mesh):

time: 133 us -> 132 us (level)
  Pallas kernels: 9.67 us -> 5.4 us
  matrix products: 0 us -> 2.65 us
    pallas_call x8 -> x9, Pallas kernels: 9.67 us -> 5.4 us  [run(): pl.pallas_call(kernel, out_shape=outs, in_specs=[IN_SMEM if i in smem els...]
    dot_general x0 -> x2, matrix products: none -> 2.65 us  [the longest x1 1.72 us: body(): jnp.einsum('hbr,bpr->bhp', third[:, :, :kv_rank], latent_cache, preferred...]
where the time goes in v4:
time: 132 us; the launch traced here: 131 us
  blocking collectives  72.9 us (55%)
  starting transfers between devices  24.7 us (19%)
  waiting for transfers between devices  22.4 us (17%)
  Pallas kernels  5.4 us (4%)
  matrix products  2.65 us (2%)
  other arithmetic  1.54 us (1%)
    all_to_all x6, blocking collectives, exchange(): return lax.all_to_all(x, axes, 0, 0, tiled=True)  72.9 us
    all_to_all x1, starting transfers between devices, exchange(): return lax.all_to_all(x, axes, 0, 0, tiled=True)  24.7 us
    all_to_all x1, waiting for transfers between devices, exchange(): return lax.all_to_all(x, axes, 0, 0, tiled=True)  22.4 us
    pallas_call x9, Pallas kernels, run(): pl.pallas_call(kernel, out_shape=outs, in_specs=[IN_SMEM if i in smem els...  5.4 us
  transfers between devices with their start and end apart: 1, of which 1 were waited for; matrix products, arithmetic and copies ran while one was open for 2% of the time, Pallas kernels for 0%

profile of v4, /device:TPU:40, one launch (start us, length us, event | category | flops | bytes accessed | tf_op | source)
XLA Modules:
  0.0 131.2 jit_solution(9497064174885225462)
XLA Ops:
  0.6 2.0 %shard_map.175 = bf16[32,40,128]{2,1,0:T(8,128)(2,1)} custom-call(bf16[8,32]{1,0:T(8,128)(2,1)} %tokens.1, f32[1,32]{1,0:T(1,128)} %bitcast.12, bf16[32,1536]{1,0:T(8,128)(2,1)} %query_down.1, bf16[32,1056]{1,0:T(8,128)(2,1)} %latent_down.1, bf16[32,512]{1,0:T(8,128)(2,1)} %key_up.1, bf16[32,512]{1,0:T(8,128)(2,1)} %value_up.1), custom_call_target="tpu_custom_call" | custom-call | tf_op jit(solution)/shard_map/pallas_call | solution.py:32
  2.6 24.7 %all-to-all-start = ((bf16[32,40,128]{2,1,0:T(8,128)(2,1)}), bf16[32,40,128]{2,1,0:T(8,128)(2,1)S(1)}, u32[]{:S(2)}, u32[]{:S(2)}) async-start(bf16[32,40,128]{2,1,0:T(8,128)(2,1)} %shard_map.175), calls=%async_computation | async-start | bytes 655360 | tf_op jit(solution)/shard_map/all_to_all | solution.py:44
  27.4 0.7 convert_element_type.16
  28.0 0.8 reshape.37
  28.8 0.8 pad_bitcast_fusion
  29.6 0.1 fusion.2
  29.7 22.4 %all-to-all-done.first = bf16[32,40,128]{2,1,0:T(8,128)(2,1)S(1)} async-done(((bf16[32,40,128]{2,1,0:T(8,128)(2,1)}), bf16[32,40,128]{2,1,0:T(8,128)(2,1)S(1)}, u32[]{:S(2)}, u32[]{:S(2)}) %all-to-all-start) | async-done | bytes 327712 | tf_op jit(solution)/shard_map/all_to_all | solution.py:44
  52.1 0.2 shard_map.176
  52.3 9.7 %all_to_all.35.refs_0_ = bf16[4,8,128]{2,1,0:T(8,128)(2,1)S(1)} all-to-all(bf16[4,8,128]{2,1,0:T(8,128)(2,1)S(1)} %get-tuple-element.13), channel_id=1, replica_groups=mesh['grp'=2,'hi'=4,'lo'=8,'tp'=4] {'tp'}, dimensions={0} | all-to-all | bytes 16384 | tf_op jit(solution)/shard_map/all_to_all | solution.py:44
  62.0 0.0 copy-done.3
  62.0 0.3 shard_map.177
  62.3 17.7 %all_to_all.36.refs_0_ = bf16[32,8,128]{2,1,0:T(8,128)(2,1)S(1)} all-to-all(bf16[32,8,128]{2,1,0:T(8,128)(2,1)S(1)} %get-tuple-element.14), channel_id=1, replica_groups=mesh['grp'=2,'hi'=4,'lo'=8,'tp'=4] {'hi','lo'}, dimensions={0} | all-to-all | bytes 131072 | tf_op jit(solution)/shard_map/all_to_all | solution.py:44
  80.1 0.0 copy-done.4
  80.1 0.3 shard_map.178
  80.4 0.0 copy-start
  80.4 0.0 copy-start.2
  80.4 9.8 %all_to_all.37.third = bf16[8,8,1280]{2,1,0:T(8,128)(2,1)S(1)} all-to-all(bf16[8,8,1280]{2,1,0:T(8,128)(2,1)S(1)} %shard_map.178), channel_id=1, replica_groups=mesh['grp'=2,'hi'=4,'lo'=8,'tp'=4] {'lo'}, dimensions={0} | all-to-all | bytes 327680 | tf_op jit(solution)/shard_map/all_to_all | solution.py:44
  90.3 0.0 slice-done
  90.3 0.0 slice-done.1
  90.3 1.7 %fusion.products = f32[8,8,384]{2,1,0:T(8,128)S(1)} fusion(bf16[8,384,1024]{2,1,0:T(8,128)(2,1)S(1)} %bitcast.11, bf16[8,8,1024]{2,1,0:T(8,128)(2,1)S(1)} %slice.4), kind=kOutput, calls=%fused_computation | convolution fusion | flops 50331648 | bytes 6520832 | tf_op jit(solution)/shard_map/hbr,bpr->bhp/dot_general | solution.py:436
  92.0 0.0 copy-done
  92.0 0.0 copy-done.2
  92.0 1.0 shard_map.179
  93.0 0.0 copy-start.1
  93.0 0.9 fusion.9.summed
  93.9 0.2 shard_map.180
  94.1 9.7 %all_to_all.38.fourth = bf16[8,8,1152]{2,1,0:T(8,128)(2,1)S(1)} all-to-all(bf16[8,8,1152]{2,1,0:T(8,128)(2,1)S(1)} %shard_map.180), channel_id=1, replica_groups=mesh['grp'=2,'hi'=4,'lo'=8,'tp'=4] {'lo'}, dimensions={0} | all-to-all | bytes 294912 | tf_op jit(solution)/shard_map/all_to_all | solution.py:44
  103.8 0.4 shard_map.181
  104.2 18.3 %all_to_all.39.fifth = bf16[32,8,128]{2,1,0:T(8,128)(2,1)S(1)} all-to-all(bf16[32,8,128]{2,1,0:T(8,128)(2,1)S(1)} %shard_map.181), channel_id=1, replica_groups=mesh['grp'=2,'hi'=4,'lo'=8,'tp'=4] {'hi','lo'}, dimensions={0} | all-to-all | bytes 131072 | tf_op jit(solution)/shard_map/all_to_all | solution.py:44
  122.4 0.4 shard_map.182
  122.9 7.7 %all_to_all.40.parts = bf16[4,8,128]{2,1,0:T(8,128)(2,1)S(1)} all-to-all(bf16[4,8,128]{2,1,0:T(8,128)(2,1)S(1)} %shard_map.182), channel_id=1, replica_groups=mesh['grp'=2,'hi'=4,'lo'=8,'tp'=4] {'tp'}, dimensions={0} | all-to-all | bytes 16384 | tf_op jit(solution)/shard_map/all_to_all | solution.py:44
  130.5 0.7 shard_map.183
  (9 shorter events, 0.0 us)
Async XLA Ops:
  2.6 49.5 %all-to-all-start = ((bf16[32,40,128]{2,1,0:T(8,128)(2,1)}), bf16[32,40,128]{2,1,0:T(8,128)(2,1)S(1)}, u32[]{:S(2)}, u32[]{:S(2)}) async-start(bf16[32,40,128]{2,1,0:T(8,128)(2,1)} %shard_map.175), calls=%async_computation | async-start | bytes 655360 | tf_op jit(solution)/shard_map/all_to_all | solution.py:44
  52.1 9.9 %copy-start.3 = (bf16[48,768]{1,0:T(8,128)(2,1)S(1)}, bf16[48,768]{1,0:T(8,128)(2,1)}, u32[]{:S(2)}) copy-start(bf16[48,768]{1,0:T(8,128)(2,1)} %refs_2_.1) | copy-start | bytes 221188
  62.0 18.1 %copy-start.4 = (f32[1024]{0:T(1024)S(1)}, f32[1024]{0:T(1024)}, u32[]{:S(2)}) copy-start(f32[1024]{0:T(1024)} %param.25) | copy-start | bytes 12292
  62.0 28.3 %slice-start = ((s8[6291456]{0:T(1024)(128)(4,1)}), s8[4194304]{0:T(1024)(128)(4,1)S(1)}, s32[]{:S(2)}) async-start(s8[6291456]{0:T(1024)(128)(4,1)} %bitcast.10), calls=%async_computation.7 | async-start | bytes 8388608
  80.1 10.2 %slice-start.1 = ((s8[6291456]{0:T(1024)(128)(4,1)}), s8[2097152]{0:T(1024)(128)(4,1)S(1)}, s32[]{:S(2)}) async-start(s8[6291456]{0:T(1024)(128)(4,1)} %bitcast.10), calls=%async_computation.8 | async-start | bytes 4194304
  80.4 11.6 %copy-start = (bf16[8,32,384]{2,1,0:T(8,128)(2,1)S(1)}, bf16[8,32,384]{2,1,0:T(8,128)(2,1)}, u32[]{:S(2)}) copy-start(bf16[8,32,384]{2,1,0:T(8,128)(2,1)} %ropes.1) | copy-start | bytes 589828
  80.4 11.6 %copy-start.2 = (s32[8]{0:T(128)S(1)}, s32[8]{0:T(128)}, u32[]{:S(2)}) copy-start(s32[8]{0:T(128)} %lengths.1) | copy-start | bytes 100
  93.0 29.4 %copy-start.1 = (bf16[512,128]{1,0:T(8,128)(2,1)S(1)}, bf16[512,128]{1,0:T(8,128)(2,1)}, u32[]{:S(2)}) copy-start(bf16[512,128]{1,0:T(8,128)(2,1)} %output_proj.1) | copy-start | bytes 393220
